TPU v7x, 32 devices: a whole 2x2x4 slice. The times are simulated.
32 devices in a mesh: gr: 2 (over core), sp: 8 (over z, y), tp: 2 (over x).
Axes of the slice: x: 2, y: 2, z: 4, core: 2. Of those that a mesh axis runs over, the one named last changes fastest.
Arguments:
- tokens: bfloat16 [4, 2048, 2048], P('gr', ('sp', 'tp')), parts along dimension 0, may hold values from -6 to 6
- key_weight: bfloat16 [2048, 1024], P('sp'), may hold values from -0.125 to 0.125
- value_weight: bfloat16 [2048, 1024], P('sp'), may hold values from -0.125 to 0.125
- queries: bfloat16 [4, 1024], P('gr'), parts along dimension 0, may hold values from -6 to 6
- head_offset: float32 [16], replicated, may hold values from -14 to -3.5
- key_bias: bfloat16 [4, 2048, 16], P('gr', ('sp', 'tp')), parts along dimension 0, may hold values from -0.5 to 12.9
Outputs:
- key_cache: bfloat16 [4, 2048, 1024], P('gr', 'sp', 'tp'), parts along dimension 0
- value_cache: bfloat16 [4, 2048, 1024], P('gr', 'sp', 'tp'), parts along dimension 0
- bias_cache: bfloat16 [4, 2048, 16], P('gr', 'sp', 'tp'), parts along dimension 0
- reading: float32 [4, 1024], P('gr', 'tp'), parts along dimension 0
There are 2 independent parts, one for each index of `gr`. A program takes and returns all parts, laid end to end along the dimension named above; an argument that names none is the same for every part. Nothing has to cross between parts.
All inputs are finite; a program needn't handle non-finite values.
Results may differ from a plain program's by a relative error of at most 0.0052.
Values may be sent and summed in bfloat16 or wider, within the bound.
A program may use at most 64 MiB of HBM per device.

v0:
```python
import functools

import jax
import jax.numpy as jnp
from jax import lax
from jax.experimental import pallas as pl
from jax.experimental.pallas import tpu as pltpu
from jax.sharding import PartitionSpec as P

MESH = pl.DeviceIdType.MESH
F32 = jnp.float32
BF16 = jnp.bfloat16
SUBS = 4


def ring_place(index, length):
    lane, row = lax.rem(index, 2), index // 2
    return row * (1 - lane) + (length - 1 - row) * lane


def ring_index(place, length):
    lane = place // (length // 2)
    row = place * (1 - lane) + (length - 1 - place) * lane
    return 2 * row + lane


def kernel(
    dims,
    tokens, key_weight, value_weight, queries, head_offset, key_bias,
    kv, bias_out, packed,
    tok, wts, acc, bias, query, offset, bias_all,
    local_sem, ring_send, ring_recv, pair_send, pair_recv,
    tok_send, tok_recv, bias_send, bias_recv, mix_send, mix_recv,
):
    n, tp_count, seqs, pos, width, rows, cols, heads, head_dim, rows_h = dims
    hops = n // 2
    sub_rows = rows // SUBS
    span = tp_count * pos
    me, tp, gr = lax.axis_index("sp"), lax.axis_index("tp"), lax.axis_index("gr")
    place = ring_place(me, n)

    def owner_at(step):
        return ring_index(lax.rem(place + step + n, n), n)

    right, left = owner_at(1), owner_at(-1)
    partner = 1 - gr
    col_start = pl.multiple_of(tp * cols, 128)
    chunked = (width // n) % 128 == 0
    order = [0]
    for h in range(1, hops + 1):
        order.extend([-h, h] if h < hops else [h])
    chunk = width // n if chunked else width
    my_rows = pl.ds(pl.multiple_of(tp * pos, pos), pos)

    weight_copies = [
        pltpu.make_async_copy(
            w.at[:, pl.ds(col_start, cols)], wts.at[part, me], local_sem.at[part]
        )
        for part, w in enumerate((key_weight, value_weight))
    ]
    tok_copy = pltpu.make_async_copy(tokens, tok.at[:, my_rows, :], local_sem.at[2])
    bias_copy = pltpu.make_async_copy(key_bias, bias_all, local_sem.at[3])
    query_copy = pltpu.make_async_copy(queries, query, local_sem.at[4])
    offset_copy = pltpu.make_async_copy(head_offset, offset, local_sem.at[5])
    for c in (*weight_copies, tok_copy, bias_copy, query_copy, offset_copy):
        c.start()

    tp_peers = [lax.rem(tp + k, tp_count) for k in range(1, tp_count)]
    barrier = pltpu.get_barrier_semaphore()
    for target in ({"sp": right}, {"sp": left}, {"gr": partner}, *({"tp": p} for p in tp_peers)):
        pl.semaphore_signal(barrier, inc=1, device_id=target, device_id_type=MESH)

    def ring_copy(direction, hop, sub, step):
        block = wts.at[gr, owner_at(step), pl.ds(sub * sub_rows, sub_rows), :]
        return pltpu.make_async_remote_copy(
            src_ref=block, dst_ref=block,
            send_sem=ring_send.at[direction, hop - 1, sub],
            recv_sem=ring_recv.at[direction, hop - 1, sub],
            device_id={"sp": right if direction == 0 else left}, device_id_type=MESH,
        )

    def step_of(direction, hop):
        return -hop if direction == 0 else hop

    def sent(direction, hop, sub):
        return ring_copy(direction, hop, sub, step_of(direction, hop - 1))

    def got(direction, hop, sub):
        return ring_copy(direction, hop, sub, step_of(direction, hop))

    def used(direction, hop, sub):
        return hop < hops or (hop == hops and sub % 2 == direction)

    def pair_copy(direction, hop, sub, part):
        block = wts.at[part, owner_at(step_of(direction, hop)), pl.ds(sub * sub_rows, sub_rows), :]
        return pltpu.make_async_remote_copy(
            src_ref=block, dst_ref=block,
            send_sem=pair_send.at[direction, hop - 1, sub],
            recv_sem=pair_recv.at[direction, hop - 1, sub],
            device_id={"gr": partner}, device_id_type=MESH,
        )

    def tok_columns(i):
        if not chunked:
            return pl.ds(0, width)
        return pl.ds(pl.multiple_of(owner_at(order[i]) * chunk, 128), chunk)

    chunk_count = len(order) if chunked else 1

    def tok_move(i, k, source):
        place_rows = pl.ds(pl.multiple_of(source * pos, pos), pos)
        block = tok.at[:, place_rows, tok_columns(i)]
        return pltpu.make_async_remote_copy(
            src_ref=block, dst_ref=block,
            send_sem=tok_send.at[i, k], recv_sem=tok_recv.at[i, k],
            device_id={"tp": lax.rem(tp + k + 1, tp_count)}, device_id_type=MESH,
        )

    def bias_move(k, source, target):
        return pltpu.make_async_remote_copy(
            src_ref=bias_all.at[:, target], dst_ref=bias.at[source],
            send_sem=bias_send.at[k], recv_sem=bias_recv.at[k],
            device_id={"tp": lax.rem(tp + k + 1, tp_count)}, device_id_type=MESH,
        )

    pl.semaphore_wait(barrier, 3 + len(tp_peers))
    for c in weight_copies:
        c.wait()
    sent_list = []

    def launch(c):
        c.start()
        sent_list.append(c)

    for sub in range(SUBS):
        for direction in range(2):
            if used(direction, 1, sub):
                launch(sent(direction, 1, sub))
    tok_copy.wait()
    for i in range(chunk_count):
        for k in range(tp_count - 1):
            launch(tok_move(i, k, tp))
    bias_copy.wait()
    for k in range(tp_count - 1):
        launch(bias_move(k, tp, lax.rem(tp + k + 1, tp_count)))
    query_copy.wait()
    offset_copy.wait()

    def tokens_ready(i):
        for k in range(tp_count - 1):
            tok_move(i, k, lax.rem(tp + tp_count - k - 1, tp_count)).wait_recv()

    def multiply(i):
        owner = owner_at(order[i])
        for part in range(2):
            w = wts[part, owner]

            def body(s, carry):
                x = tok[s, :, tok_columns(i)]
                y = jnp.dot(x, w, preferred_element_type=F32)
                if i > 0:
                    y = acc[part, s] + y
                acc[part, s] = y
                return carry

            lax.fori_loop(0, seqs, body, 0)

    def close(i, source):
        owner = owner_at(order[i])
        where = pl.ds(pl.multiple_of(source * pos, pos), pos)
        for part in range(2):
            for s in range(seqs):
                y = jnp.dot(
                    tok[s, where, tok_columns(i)], wts[part, owner], preferred_element_type=F32
                )
                kv[part, s, where, :] = (acc[part, s, where, :] + y).astype(BF16)

    def pair_ready(hop):
        for direction in range(2):
            for sub in range(SUBS):
                if used(direction, hop, sub):
                    pair_copy(direction, hop, sub, partner).wait_recv()

    def steps_of_hop(hop):
        if hop == 0:
            return [0]
        first = 1 + 2 * (hop - 1)
        return [first, first + 1] if hop < hops else [first]

    def compute_hop(hop):
        if hop > 0:
            pair_ready(hop)
        if chunked:
            for i in steps_of_hop(hop):
                if i < len(order) - 1:
                    tokens_ready(i)
                    multiply(i)
                else:
                    close(i, tp)
                    tokens_ready(i)
                    for p in tp_peers:
                        close(i, p)

    for hop in range(1, hops + 1):
        for sub in range(SUBS):
            for direction in range(2):
                if not used(direction, hop, sub):
                    continue
                got(direction, hop, sub).wait_recv()
                if hop < hops and used(direction, hop + 1, sub):
                    launch(sent(direction, hop + 1, sub))
                launch(pair_copy(direction, hop, sub, gr))
        compute_hop(hop - 1)
    compute_hop(hops)

    if not chunked:
        tokens_ready(0)
        tile = pos
        for part in range(2):
            w = wts[part].reshape(width, cols)

            def body(j, carry):
                s, r = j // (span // tile), lax.rem(j, span // tile)
                where = pl.ds(pl.multiple_of(r * tile, tile), tile)
                y = jnp.dot(tok[s, where, :], w, preferred_element_type=F32)
                kv[part, s, where, :] = y.astype(BF16)
                return carry

            lax.fori_loop(0, seqs * (span // tile), body, 0)

    for k in range(tp_count - 1):
        bias_move(k, lax.rem(tp + tp_count - k - 1, tp_count), tp).wait_recv()
    bias[tp] = bias_all[:, tp]

    row_id = lax.broadcasted_iota(jnp.int32, (rows_h, cols), 0)
    col_id = lax.broadcasted_iota(jnp.int32, (rows_h, cols), 1)
    own = row_id == col_id // head_dim
    q = query[:, pl.ds(col_start, cols)].astype(F32)
    total_heads = offset.shape[1]
    pick = lax.broadcasted_iota(jnp.int32, (rows_h, total_heads), 1) == (
        lax.broadcasted_iota(jnp.int32, (rows_h, total_heads), 0) + tp * heads
    )
    offset_col = jnp.sum(jnp.where(pick, offset[...], 0.0), axis=1, keepdims=True)
    logits = []
    for s in range(seqs):
        q_rows = jnp.where(own, q[s : s + 1], 0.0).astype(BF16)
        b = jnp.concatenate([bias[t, s] for t in range(tp_count)], axis=1)
        bias_out[s] = b
        b = b.astype(F32)
        if rows_h > heads:
            b = jnp.concatenate([b, jnp.zeros((rows_h - heads, span), F32)], axis=0)
        logits.append(
            lax.dot_general(
                q_rows, kv[0, s], (((1,), (1,)), ((), ())), preferred_element_type=F32
            )
            * (head_dim**-0.5)
            + offset_col
            + b
        )
    logits = jnp.concatenate(logits, axis=0)
    soft = jnp.log1p(jnp.exp(-jnp.abs(logits)))
    fading = -jnp.maximum(logits, 0.0) - soft
    taking = jnp.minimum(logits, 0.0) - soft
    high = fading.astype(BF16)
    rest = fading - high.astype(F32)
    mid = rest.astype(BF16)
    low = (rest - mid.astype(F32)).astype(BF16)
    later = (
        lax.broadcasted_iota(jnp.int32, (span, span), 0)
        > lax.broadcasted_iota(jnp.int32, (span, span), 1)
    ).astype(F32).astype(BF16)
    sums = jnp.dot(
        jnp.concatenate([high, mid, low], axis=0), later, preferred_element_type=F32
    )
    m = seqs * rows_h
    within = sums[:m] + sums[m : 2 * m] + sums[2 * m :]
    weights = jnp.exp(taking + within).astype(BF16)
    totals = jnp.sum(fading, axis=1, keepdims=True)
    for s in range(seqs):
        at = slice(s * rows_h, (s + 1) * rows_h)
        partial = jnp.dot(weights[at], kv[1, s], preferred_element_type=F32)
        packed[me, s : s + 1] = jnp.sum(jnp.where(own, partial, 0.0), axis=0, keepdims=True)
        packed[me, seqs + s : seqs + s + 1] = jnp.sum(
            jnp.where(own, totals[at], 0.0), axis=0, keepdims=True
        )

    def mix_move(k, source):
        return pltpu.make_async_remote_copy(
            src_ref=packed.at[source], dst_ref=packed.at[source],
            send_sem=mix_send.at[k - 1], recv_sem=mix_recv.at[k - 1],
            device_id={"sp": lax.rem(me + k, n)}, device_id_type=MESH,
        )

    for k in range(1, n):
        launch(mix_move(k, me))
    for k in range(1, n):
        mix_move(k, lax.rem(me + n - k, n)).wait_recv()
    for c in sent_list:
        c.wait_send()


def finish(n, head_dim, kv, bias, packed, key_out, value_out, bias_out, reading_out, sems):
    moves = [
        pltpu.make_async_copy(kv.at[0], key_out, sems.at[0]),
        pltpu.make_async_copy(kv.at[1], value_out, sems.at[1]),
        pltpu.make_async_copy(bias, bias_out, sems.at[2]),
    ]
    for c in moves:
        c.start()
    seqs, cols = reading_out.shape
    rows_h = max(8, cols // head_dim)
    row_id = lax.broadcasted_iota(jnp.int32, (rows_h, cols), 0)
    col_id = lax.broadcasted_iota(jnp.int32, (rows_h, cols), 1)
    own = row_id == col_id // head_dim
    mixture = jnp.zeros((seqs, cols), F32)
    carry = jnp.zeros((seqs, cols), F32)
    for at in range(n - 1, -1, -1):
        mixture = mixture + jnp.exp(carry) * packed[at, :seqs]
        carry = carry + packed[at, seqs:]
    for s in range(seqs):
        x = mixture[s : s + 1]
        mean = jnp.sum(jnp.where(own, x * x, 0.0), axis=1, keepdims=True) / head_dim
        scale = jnp.sum(jnp.where(own, lax.rsqrt(mean + 1e-06), 0.0), axis=0, keepdims=True)
        reading_out[s : s + 1] = x * scale
    for c in moves:
        c.wait()


def per_device(tokens, key_weight, value_weight, queries, head_offset, key_bias):
    n, tp_count = lax.axis_size("sp"), lax.axis_size("tp")
    assert n % 2 == 0 and lax.axis_size("gr") == 2
    seqs, pos, width = tokens.shape
    rows, kv_width = key_weight.shape
    head_count = head_offset.shape[0]
    head_dim = kv_width // head_count
    cols = kv_width // tp_count
    heads = head_count // tp_count
    rows_h = max(8, heads)
    span = tp_count * pos
    hops = n // 2
    bias_rows = jnp.transpose(key_bias, (0, 2, 1)).reshape(seqs, tp_count, heads, pos)
    dims = (n, tp_count, seqs, pos, width, rows, cols, heads, head_dim, rows_h)
    peers = max(tp_count - 1, 1)
    chunks = n if (width // n) % 128 == 0 else 1
    dma = pltpu.SemaphoreType.DMA
    kv, bias_held, packed = pl.pallas_call(
        functools.partial(kernel, dims),
        out_shape=(
            jax.ShapeDtypeStruct((2, seqs, span, cols), BF16),
            jax.ShapeDtypeStruct((seqs, heads, span), BF16),
            jax.ShapeDtypeStruct((n, 2 * seqs, cols), F32),
        ),
        in_specs=[pl.BlockSpec(memory_space=pltpu.HBM)] * 6,
        out_specs=[pl.BlockSpec(memory_space=pltpu.VMEM)] * 3,
        scratch_shapes=[
            pltpu.VMEM((seqs, span, width), BF16),
            pltpu.VMEM((2, n, rows, cols), BF16),
            pltpu.VMEM((2, seqs, span, cols), F32),
            pltpu.VMEM((tp_count, seqs, heads, pos), BF16),
            pltpu.VMEM(queries.shape, BF16),
            pltpu.VMEM((1, head_count), F32),
            pltpu.VMEM((seqs, tp_count, heads, pos), BF16),
            dma((6,)),
            dma((2, hops, SUBS)),
            dma((2, hops, SUBS)),
            dma((2, hops, SUBS)),
            dma((2, hops, SUBS)),
            dma((chunks, peers)),
            dma((chunks, peers)),
            dma((peers,)),
            dma((peers,)),
            dma((n - 1,)),
            dma((n - 1,)),
        ],
        compiler_params=pltpu.CompilerParams(
            collective_id=0, has_side_effects=True, vmem_limit_bytes=36 * 2**20
        ),
        name="prefill",
    )(*(pltpu.with_memory_space_constraint(a, pltpu.HBM) for a in (tokens, key_weight, value_weight, queries, head_offset.reshape(1, head_count), bias_rows)))
    key_cache, value_cache, bias_cache, reading = pl.pallas_call(
        functools.partial(finish, n, head_dim),
        out_shape=(
            jax.ShapeDtypeStruct((seqs, span, cols), BF16),
            jax.ShapeDtypeStruct((seqs, span, cols), BF16),
            jax.ShapeDtypeStruct((seqs, heads, span), BF16),
            jax.ShapeDtypeStruct((seqs, cols), F32),
        ),
        in_specs=[
            pl.BlockSpec(memory_space=pl.ANY),
            pl.BlockSpec(memory_space=pl.ANY),
            pl.BlockSpec(memory_space=pltpu.VMEM),
        ],
        out_specs=[
            pl.BlockSpec(memory_space=pl.ANY),
            pl.BlockSpec(memory_space=pl.ANY),
            pl.BlockSpec(memory_space=pl.ANY),
            pl.BlockSpec(memory_space=pltpu.VMEM),
        ],
        scratch_shapes=[dma((3,))],
        compiler_params=pltpu.CompilerParams(vmem_limit_bytes=4 * 2**20),
        name="finish",
    )(kv, bias_held, packed)
    return key_cache, value_cache, jnp.transpose(bias_cache, (0, 2, 1)), reading


def solution(mesh):
    in_specs = (
        P("gr", ("sp", "tp"), None),
        P("sp", None),
        P("sp", None),
        P("gr", None),
        P(),
        P("gr", ("sp", "tp"), None),
    )
    out_specs = (P("gr", "sp", "tp"), P("gr", "sp", "tp"), P("gr", "sp", "tp"), P("gr", "tp"))
    return jax.shard_map(
        per_device, mesh=mesh, in_specs=in_specs, out_specs=out_specs, check_vma=False
    )
```

profile of v0, /device:TPU:0, one launch (start us, length us, event | category | flops | bytes accessed | tf_op | source)
XLA Modules:
  0.0 38.8 jit_solution(9384247984358644111)
XLA Ops:
  0.6 36.6 %prefill.1 = (bf16[2,2,256,512]{3,2,1,0:T(8,128)(2,1)S(1)}, bf16[2,8,256]{2,1,0:T(8,128)(2,1)S(1)}, f32[8,4,512]{2,1,0:T(4,128)S(1)}) custom-call(bf16[2,128,2048]{2,1,0:T(8,128)(2,1)} %tokens.1, bf16[256,1024]{1,0:T(8,128)(2,1)} %key_weight.1, bf16[256,1024]{1,0:T(8,128)(2,1)} %value_weight.1, bf16[2,1024]{1,0:T(2,128)(2,1)} %queries.1, f32[1,16]{1,0:T(1,128)} %bitcast.6, ...), custom_call_target="tpu_custom_call" | custom-call | tf_op jit(solution)/shard_map/prefill/pallas_call | solution.py:346
  37.2 1.6 %finish.1 = (bf16[2,256,512]{2,1,0:T(8,128)(2,1)}, bf16[2,256,512]{2,1,0:T(8,128)(2,1)}, bf16[2,8,256]{2,1,0:T(8,128)(2,1)}, f32[2,512]{1,0:T(2,128)}) custom-call(bf16[2,2,256,512]{3,2,1,0:T(8,128)(2,1)S(1)} %get-tuple-element.11.kv, bf16[2,8,256]{2,1,0:T(8,128)(2,1)S(1)} %get-tuple-element.12.bias, f32[8,4,512]{2,1,0:T(4,128)S(1)} %get-tuple-element.13.packed), custom_call_target="tpu_custom_call" | custom-call | tf_op jit(solution)/shard_map/finish/pallas_call | solution.py:380
where the time goes:
time: 39 us; the launch traced here: 38.8 us
  Pallas kernels  38.2 us (98%)
  between operations  0.64 us (2%)
    pallas_call x1, Pallas kernels, per_device(): pl.pallas_call(functools.partial(kernel, dims), out_shape=(jax.ShapeDtype...  36.6 us
    pallas_call x1, Pallas kernels, per_device(): pl.pallas_call(functools.partial(finish, n, head_dim), out_shape=(jax.Sha...  1.6 us

commit v1 on v0

v1 whole, which is shorter than its diff:
```python
import functools

import jax
import jax.numpy as jnp
from jax import lax
from jax.experimental import pallas as pl
from jax.experimental.pallas import tpu as pltpu
from jax.sharding import PartitionSpec as P

MESH = pl.DeviceIdType.MESH
F32 = jnp.float32
BF16 = jnp.bfloat16
SUBS = 2
MARK = 2 * SUBS
AHEAD = 2
MIX_HOP = 2


def ring_place(index, length):
    lane, row = lax.rem(index, 2), index // 2
    return row * (1 - lane) + (length - 1 - row) * lane


def ring_index(place, length):
    lane = place // (length // 2)
    row = place * (1 - lane) + (length - 1 - place) * lane
    return 2 * row + lane


def kernel(
    dims,
    tokens, key_weight, value_weight, queries, head_offset, key_bias, own_bias,
    kv, bias_out, packed,
    tok, wts, acc, bias, query, offset, bias_all, bias_own, key_rows,
    ubuf, ucat, pout, pin, plow, tot_out, tot_in,
    local_sem, ring_send, ring_recv, pair_send, pair_recv,
    tok_send, tok_recv, bias_send, bias_recv, read_send, read_recv, mix_send, mix_recv,
):
    n, tp_count, seqs, pos, width, rows, cols, heads, head_dim, rows_h = dims
    hops = n // 2
    half_rows = rows // 2
    sub_rows = half_rows // SUBS
    span = tp_count * pos
    kv_width = tp_count * cols
    me, tp, gr = lax.axis_index("sp"), lax.axis_index("tp"), lax.axis_index("gr")
    place = ring_place(me, n)

    def owner_at(step):
        return ring_index(lax.rem(place + step + n, n), n)

    right, left = owner_at(1), owner_at(-1)
    partner = 1 - gr
    col_start = pl.multiple_of(tp * cols, 128)
    chunked = (width // n) % 128 == 0
    order = [0]
    for h in range(1, hops + 1):
        order.extend([-h, h] if h < hops else [h])
    chunk = width // n if chunked else width
    my_rows = pl.ds(pl.multiple_of(tp * pos, pos), pos)

    key_copy = pltpu.make_async_copy(key_weight, key_rows, local_sem.at[6])
    query_copy = pltpu.make_async_copy(queries, query, local_sem.at[4])
    weight_copies = [
        pltpu.make_async_copy(
            w.at[:, pl.ds(col_start, cols)], wts.at[part, me], local_sem.at[part]
        )
        for part, w in enumerate((key_weight, value_weight))
    ]
    tok_copy = pltpu.make_async_copy(tokens, tok.at[:, my_rows, :], local_sem.at[2])
    bias_copy = pltpu.make_async_copy(key_bias, bias_all, local_sem.at[3])
    own_bias_copy = pltpu.make_async_copy(own_bias, bias_own, local_sem.at[7])
    offset_copy = pltpu.make_async_copy(head_offset, offset, local_sem.at[5])
    for c in (
        weight_copies[1], tok_copy, query_copy, key_copy, weight_copies[0],
        bias_copy, own_bias_copy, offset_copy,
    ):
        c.start()

    tp_peers = [lax.rem(tp + k, tp_count) for k in range(1, tp_count)]
    barrier = pltpu.get_barrier_semaphore()
    for target in ({"sp": right}, {"sp": left}, {"gr": partner}, *({"tp": p} for p in tp_peers)):
        pl.semaphore_signal(barrier, inc=1, device_id=target, device_id_type=MESH)

    def part_of(piece):
        return 1 if piece < SUBS else 0

    def rows_of(piece, core):
        return pl.ds(pl.multiple_of(core * half_rows + (piece % SUBS) * sub_rows, sub_rows), sub_rows)

    def block_of(piece, step, core):
        if piece == MARK:
            return ubuf.at[owner_at(step)]
        return wts.at[part_of(piece), owner_at(step), rows_of(piece, core), :]

    def ring_copy(direction, hop, piece, step):
        block = block_of(piece, step, gr)
        return pltpu.make_async_remote_copy(
            src_ref=block, dst_ref=block,
            send_sem=ring_send.at[direction, hop - 1, piece],
            recv_sem=ring_recv.at[direction, hop - 1, piece],
            device_id={"sp": right if direction == 0 else left}, device_id_type=MESH,
        )

    def step_of(direction, hop):
        return -hop if direction == 0 else hop

    def sent(direction, hop, piece):
        return ring_copy(direction, hop, piece, step_of(direction, hop - 1))

    def got(direction, hop, piece):
        return ring_copy(direction, hop, piece, step_of(direction, hop))

    def used(direction, hop, piece):
        return hop < hops or (hop == hops and piece % 2 == direction)

    def pair_copy(direction, hop, piece, core):
        block = block_of(piece, step_of(direction, hop), core)
        return pltpu.make_async_remote_copy(
            src_ref=block, dst_ref=block,
            send_sem=pair_send.at[direction, hop - 1, piece],
            recv_sem=pair_recv.at[direction, hop - 1, piece],
            device_id={"gr": partner}, device_id_type=MESH,
        )

    def tok_columns(i):
        if not chunked:
            return pl.ds(0, width)
        return pl.ds(pl.multiple_of(owner_at(order[i]) * chunk, 128), chunk)

    chunk_count = len(order) if chunked else 1

    def peer_of(k):
        return lax.rem(tp + k + 1, tp_count)

    def source_of(k):
        return lax.rem(tp + tp_count - k - 1, tp_count)

    def tok_move(i, k, source):
        place_rows = pl.ds(pl.multiple_of(source * pos, pos), pos)
        block = tok.at[:, place_rows, tok_columns(i)]
        return pltpu.make_async_remote_copy(
            src_ref=block, dst_ref=block,
            send_sem=tok_send.at[i, k], recv_sem=tok_recv.at[i, k],
            device_id={"tp": peer_of(k)}, device_id_type=MESH,
        )

    def bias_move(k, source, target):
        return pltpu.make_async_remote_copy(
            src_ref=bias_all.at[:, target], dst_ref=bias.at[source],
            send_sem=bias_send.at[k], recv_sem=bias_recv.at[k],
            device_id={"tp": peer_of(k)}, device_id_type=MESH,
        )

    def read_move(k, which, source, target):
        out, into = ((pout, pin), (tot_out, tot_in))[which]
        return pltpu.make_async_remote_copy(
            src_ref=out.at[target], dst_ref=into.at[source],
            send_sem=read_send.at[which, k], recv_sem=read_recv.at[which, k],
            device_id={"tp": peer_of(k)}, device_id_type=MESH,
        )

    sent_list = []

    def launch(c):
        c.start()
        sent_list.append(c)

    issued = [0]

    def send_tokens(upto):
        while issued[0] < min(upto, chunk_count):
            for k in range(tp_count - 1):
                launch(tok_move(issued[0], k, tp))
            issued[0] += 1

    def open_ring(piece):
        for direction in range(2):
            if used(direction, 1, piece):
                launch(sent(direction, 1, piece))

    def pass_on(hop, pieces):
        for piece in pieces:
            for direction in range(2):
                if not used(direction, hop, piece):
                    continue
                got(direction, hop, piece).wait_recv()
                if hop < hops and used(direction, hop + 1, piece):
                    launch(sent(direction, hop + 1, piece))
                if piece != MARK:
                    launch(pair_copy(direction, hop, piece, gr))

    value_pieces = list(range(SUBS))
    key_pieces = list(range(SUBS, 2 * SUBS))
    first_pass = value_pieces[:1] + [MARK] + value_pieces[1:]

    pl.semaphore_wait(barrier, 3 + len(tp_peers))
    weight_copies[1].wait()
    open_ring(value_pieces[0])
    tok_copy.wait()
    send_tokens(AHEAD)

    query_copy.wait()
    key_copy.wait()
    group = tp_count * rows_h
    row = lax.broadcasted_iota(jnp.int32, (group, kv_width), 0)
    col_head = lax.broadcasted_iota(jnp.int32, (group, kv_width), 1) // head_dim
    inner = lax.rem(row, rows_h)
    mine = (row // rows_h * heads + inner == col_head) & (inner < heads)
    q = query[...].astype(F32)
    q_rows = jnp.concatenate(
        [jnp.where(mine, q[s : s + 1], 0.0) for s in range(seqs)], axis=0
    ).astype(BF16)
    ubuf[me] = lax.dot_general(
        q_rows, key_rows[...], (((1,), (1,)), ((), ())), preferred_element_type=F32
    ).astype(BF16)
    for piece in value_pieces[1:]:
        open_ring(piece)
    open_ring(MARK)
    bias_copy.wait()
    for k in range(tp_count - 1):
        launch(bias_move(k, tp, peer_of(k)))
    weight_copies[0].wait()
    own_bias_copy.wait()
    offset_copy.wait()

    for hop in range(1, hops + 1):
        pass_on(hop, first_pass)
        send_tokens(AHEAD + hop)
        if hop == max(hops - 1, 1):
            for piece in key_pieces:
                open_ring(piece)

    for owner in range(n):
        ucat[:, owner * rows : (owner + 1) * rows] = ubuf[owner]
    total_heads = offset.shape[1]
    pick_row = lax.broadcasted_iota(jnp.int32, (group, total_heads), 0)
    pick_inner = lax.rem(pick_row, rows_h)
    pick = (
        lax.broadcasted_iota(jnp.int32, (group, total_heads), 1)
        == pick_row // rows_h * heads + pick_inner
    ) & (pick_inner < heads)
    offset_col = jnp.sum(jnp.where(pick, offset[...], 0.0), axis=1, keepdims=True)
    logits = []
    for s in range(seqs):
        logits.append(
            lax.dot_general(
                ucat[s * group : (s + 1) * group, :], tok[s, my_rows, :],
                (((1,), (1,)), ((), ())), preferred_element_type=F32,
            )
            * (head_dim**-0.5)
            + offset_col
            + bias_own[s].astype(F32)
        )
    logits = jnp.concatenate(logits, axis=0)
    soft = jnp.log1p(jnp.exp(-jnp.abs(logits)))
    fading = -jnp.maximum(logits, 0.0) - soft
    taking = jnp.minimum(logits, 0.0) - soft
    high = fading.astype(BF16)
    rest = fading - high.astype(F32)
    mid = rest.astype(BF16)
    low = (rest - mid.astype(F32)).astype(BF16)
    later = (
        lax.broadcasted_iota(jnp.int32, (pos, pos), 0)
        > lax.broadcasted_iota(jnp.int32, (pos, pos), 1)
    ).astype(F32).astype(BF16)
    sums = jnp.dot(
        jnp.concatenate([high, mid, low], axis=0), later, preferred_element_type=F32
    )
    m = seqs * group
    within = sums[:m] + sums[m : 2 * m] + sums[2 * m :]
    weights = jnp.exp(taking + within).astype(BF16)
    totals = jnp.sum(fading, axis=1, keepdims=True)
    spread = jnp.broadcast_to(totals, (m, 128))
    weighted = [
        jnp.dot(
            weights[s * group : (s + 1) * group], tok[s, my_rows, :],
            preferred_element_type=F32,
        )
        for s in range(seqs)
    ]
    lows = []
    for t in range(tp_count):
        at = slice(t * rows_h, (t + 1) * rows_h)
        tot_out[t] = jnp.concatenate(
            [spread[s * group + t * rows_h : s * group + (t + 1) * rows_h] for s in range(seqs)],
            axis=0,
        )
        whole = jnp.concatenate([weighted[s][at] for s in range(seqs)], axis=0)
        upper = whole.astype(BF16)
        pout[t] = upper
        plow[t] = (whole - upper.astype(F32)).astype(BF16)
    for k in range(tp_count - 1):
        for which in range(2):
            launch(read_move(k, which, tp, peer_of(k)))
    pin[tp] = pout[tp]
    tot_in[tp] = tot_out[tp]
    send_tokens(chunk_count)

    def pair_ready(hop, pieces):
        for direction in range(2):
            for piece in pieces:
                if used(direction, hop, piece):
                    pair_copy(direction, hop, piece, partner).wait_recv()

    for hop in range(1, hops + 1):
        pair_ready(hop, value_pieces)

    def tokens_ready(i):
        for k in range(tp_count - 1):
            tok_move(i, k, source_of(k)).wait_recv()

    def multiply(i):
        owner = owner_at(order[i])
        for part in range(2):
            w = wts[part, owner]

            def body(s, carry):
                x = tok[s, :, tok_columns(i)]
                y = jnp.dot(x, w, preferred_element_type=F32)
                if i > 0:
                    y = acc[part, s] + y
                acc[part, s] = y
                return carry

            lax.fori_loop(0, seqs, body, 0)

    def close(i, source):
        owner = owner_at(order[i])
        where = pl.ds(pl.multiple_of(source * pos, pos), pos)
        for part in range(2):
            for s in range(seqs):
                y = jnp.dot(
                    tok[s, where, tok_columns(i)], wts[part, owner], preferred_element_type=F32
                )
                kv[part, s, where, :] = (acc[part, s, where, :] + y).astype(BF16)

    def steps_of_hop(hop):
        if hop == 0:
            return [0]
        first = 1 + 2 * (hop - 1)
        return [first, first + 1] if hop < hops else [first]

    def compute_hop(hop):
        if hop > 0:
            pair_ready(hop, key_pieces)
        if chunked:
            for i in steps_of_hop(hop):
                if i < len(order) - 1:
                    tokens_ready(i)
                    multiply(i)
                else:
                    close(i, tp)
                    tokens_ready(i)
                    for p in tp_peers:
                        close(i, p)

    def mix_move(k, source):
        return pltpu.make_async_remote_copy(
            src_ref=packed.at[source], dst_ref=packed.at[source],
            send_sem=mix_send.at[k - 1], recv_sem=mix_recv.at[k - 1],
            device_id={"sp": lax.rem(me + k, n)}, device_id_type=MESH,
        )

    def mix():
        for k in range(tp_count - 1):
            for which in range(2):
                read_move(k, which, source_of(k), tp).wait_recv()
        count = seqs * rows_h
        given = jnp.concatenate([pin[t] for t in range(tp_count)] + [plow[tp]], axis=0)
        product = jnp.dot(
            given, wts[1].reshape(width, cols), preferred_element_type=F32
        )
        carry = jnp.zeros((count, 1), F32)
        mixture = jnp.zeros((count, cols), F32)
        for t in range(tp_count - 1, -1, -1):
            term = product[t * count : (t + 1) * count]
            term = term + jnp.where(tp == t, 1.0, 0.0) * product[tp_count * count :]
            mixture = mixture + jnp.exp(carry) * term
            carry = carry + tot_in[t][:, :1]
        own = lax.broadcasted_iota(jnp.int32, (rows_h, cols), 0) == (
            lax.broadcasted_iota(jnp.int32, (rows_h, cols), 1) // head_dim
        )
        for s in range(seqs):
            at = slice(s * rows_h, (s + 1) * rows_h)
            packed[me, s : s + 1] = jnp.sum(
                jnp.where(own, mixture[at], 0.0), axis=0, keepdims=True
            )
            packed[me, seqs + s : seqs + s + 1] = jnp.sum(
                jnp.where(own, carry[at], 0.0), axis=0, keepdims=True
            )
        for k in range(1, n):
            launch(mix_move(k, me))

    for hop in range(1, hops + 1):
        pass_on(hop, key_pieces)
        if hop == min(MIX_HOP, hops):
            mix()
        compute_hop(hop - 1)
    compute_hop(hops)

    if not chunked:
        tokens_ready(0)
        tile = pos
        for part in range(2):
            w = wts[part].reshape(width, cols)

            def body(j, carry):
                s, r = j // (span // tile), lax.rem(j, span // tile)
                where = pl.ds(pl.multiple_of(r * tile, tile), tile)
                y = jnp.dot(tok[s, where, :], w, preferred_element_type=F32)
                kv[part, s, where, :] = y.astype(BF16)
                return carry

            lax.fori_loop(0, seqs * (span // tile), body, 0)

    for k in range(tp_count - 1):
        bias_move(k, source_of(k), tp).wait_recv()
    bias[tp] = bias_all[:, tp]
    for s in range(seqs):
        bias_out[s] = jnp.concatenate([bias[t, s] for t in range(tp_count)], axis=1)
    for k in range(1, n):
        mix_move(k, lax.rem(me + n - k, n)).wait_recv()
    for c in sent_list:
        c.wait_send()


def finish(n, head_dim, kv, bias, packed, key_out, value_out, bias_out, reading_out, sems):
    moves = [
        pltpu.make_async_copy(kv.at[0], key_out, sems.at[0]),
        pltpu.make_async_copy(kv.at[1], value_out, sems.at[1]),
        pltpu.make_async_copy(bias, bias_out, sems.at[2]),
    ]
    for c in moves:
        c.start()
    seqs, cols = reading_out.shape
    rows_h = max(8, cols // head_dim)
    row_id = lax.broadcasted_iota(jnp.int32, (rows_h, cols), 0)
    col_id = lax.broadcasted_iota(jnp.int32, (rows_h, cols), 1)
    own = row_id == col_id // head_dim
    mixture = jnp.zeros((seqs, cols), F32)
    carry = jnp.zeros((seqs, cols), F32)
    for at in range(n - 1, -1, -1):
        mixture = mixture + jnp.exp(carry) * packed[at, :seqs]
        carry = carry + packed[at, seqs:]
    for s in range(seqs):
        x = mixture[s : s + 1]
        mean = jnp.sum(jnp.where(own, x * x, 0.0), axis=1, keepdims=True) / head_dim
        scale = jnp.sum(jnp.where(own, lax.rsqrt(mean + 1e-06), 0.0), axis=0, keepdims=True)
        reading_out[s : s + 1] = x * scale
    for c in moves:
        c.wait()


def per_device(tokens, key_weight, value_weight, queries, head_offset, key_bias):
    n, tp_count = lax.axis_size("sp"), lax.axis_size("tp")
    assert n % 2 == 0 and lax.axis_size("gr") == 2
    seqs, pos, width = tokens.shape
    rows, kv_width = key_weight.shape
    head_count = head_offset.shape[0]
    head_dim = kv_width // head_count
    cols = kv_width // tp_count
    heads = head_count // tp_count
    rows_h = max(8, heads)
    span = tp_count * pos
    hops = n // 2
    bias_rows = jnp.transpose(key_bias, (0, 2, 1)).reshape(seqs, tp_count, heads, pos)
    group = tp_count * rows_h
    own_bias = jnp.pad(bias_rows, ((0, 0), (0, 0), (0, rows_h - heads), (0, 0)))
    own_bias = own_bias.reshape(seqs, group, pos)
    dims = (n, tp_count, seqs, pos, width, rows, cols, heads, head_dim, rows_h)
    peers = max(tp_count - 1, 1)
    chunks = n if (width // n) % 128 == 0 else 1
    dma = pltpu.SemaphoreType.DMA
    kv, bias_held, packed = pl.pallas_call(
        functools.partial(kernel, dims),
        out_shape=(
            jax.ShapeDtypeStruct((2, seqs, span, cols), BF16),
            jax.ShapeDtypeStruct((seqs, heads, span), BF16),
            jax.ShapeDtypeStruct((n, 2 * seqs, cols), F32),
        ),
        in_specs=[pl.BlockSpec(memory_space=pltpu.HBM)] * 7,
        out_specs=[pl.BlockSpec(memory_space=pltpu.VMEM)] * 3,
        scratch_shapes=[
            pltpu.VMEM((seqs, span, width), BF16),
            pltpu.VMEM((2, n, rows, cols), BF16),
            pltpu.VMEM((2, seqs, span, cols), F32),
            pltpu.VMEM((tp_count, seqs, heads, pos), BF16),
            pltpu.VMEM(queries.shape, BF16),
            pltpu.VMEM((1, head_count), F32),
            pltpu.VMEM((seqs, tp_count, heads, pos), BF16),
            pltpu.VMEM((seqs, group, pos), BF16),
            pltpu.VMEM((rows, kv_width), BF16),
            pltpu.VMEM((n, seqs * group, rows), BF16),
            pltpu.VMEM((seqs * group, width), BF16),
            pltpu.VMEM((tp_count, seqs * rows_h, width), BF16),
            pltpu.VMEM((tp_count, seqs * rows_h, width), BF16),
            pltpu.VMEM((tp_count, seqs * rows_h, width), BF16),
            pltpu.VMEM((tp_count, seqs * rows_h, 128), F32),
            pltpu.VMEM((tp_count, seqs * rows_h, 128), F32),
            dma((8,)),
            dma((2, hops, MARK + 1)),
            dma((2, hops, MARK + 1)),
            dma((2, hops, MARK + 1)),
            dma((2, hops, MARK + 1)),
            dma((chunks, peers)),
            dma((chunks, peers)),
            dma((peers,)),
            dma((peers,)),
            dma((2, peers)),
            dma((2, peers)),
            dma((n - 1,)),
            dma((n - 1,)),
        ],
        compiler_params=pltpu.CompilerParams(
            collective_id=0, has_side_effects=True, vmem_limit_bytes=36 * 2**20
        ),
        name="prefill",
    )(*(pltpu.with_memory_space_constraint(a, pltpu.HBM) for a in (tokens, key_weight, value_weight, queries, head_offset.reshape(1, head_count), bias_rows, own_bias)))
    key_cache, value_cache, bias_cache, reading = pl.pallas_call(
        functools.partial(finish, n, head_dim),
        out_shape=(
            jax.ShapeDtypeStruct((seqs, span, cols), BF16),
            jax.ShapeDtypeStruct((seqs, span, cols), BF16),
            jax.ShapeDtypeStruct((seqs, heads, span), BF16),
            jax.ShapeDtypeStruct((seqs, cols), F32),
        ),
        in_specs=[
            pl.BlockSpec(memory_space=pl.ANY),
            pl.BlockSpec(memory_space=pl.ANY),
            pl.BlockSpec(memory_space=pltpu.VMEM),
        ],
        out_specs=[
            pl.BlockSpec(memory_space=pl.ANY),
            pl.BlockSpec(memory_space=pl.ANY),
            pl.BlockSpec(memory_space=pl.ANY),
            pl.BlockSpec(memory_space=pltpu.VMEM),
        ],
        scratch_shapes=[dma((3,))],
        compiler_params=pltpu.CompilerParams(vmem_limit_bytes=4 * 2**20),
        name="finish",
    )(kv, bias_held, packed)
    return key_cache, value_cache, jnp.transpose(bias_cache, (0, 2, 1)), reading


def solution(mesh):
    in_specs = (
        P("gr", ("sp", "tp"), None),
        P("sp", None),
        P("sp", None),
        P("gr", None),
        P(),
        P("gr", ("sp", "tp"), None),
    )
    out_specs = (P("gr", "sp", "tp"), P("gr", "sp", "tp"), P("gr", "sp", "tp"), P("gr", "tp"))
    return jax.shard_map(
        per_device, mesh=mesh, in_specs=in_specs, out_specs=out_specs, check_vma=False
    )
```

time: 39 us -> 41.5 us (1.064)
  Pallas kernels: 38.2 us -> 40.7 us
    pallas_call x1, Pallas kernels: 36.6 us -> 39.1 us  [per_device(): pl.pallas_call(functools.partial(kernel, dims), out_shape=(jax.ShapeDtype...]
where the time goes in v1:
time: 41.5 us; the launch traced here: 41.3 us
  Pallas kernels  40.7 us (98%)
  between operations  0.64 us (2%)
    pallas_call x1, Pallas kernels, per_device(): pl.pallas_call(functools.partial(kernel, dims), out_shape=(jax.ShapeDtype...  39.1 us
    pallas_call x1, Pallas kernels, per_device(): pl.pallas_call(functools.partial(finish, n, head_dim), out_shape=(jax.Sha...  1.6 us

profile of v1, /device:TPU:0, one launch (start us, length us, event | category | flops | bytes accessed | tf_op | source)
XLA Modules:
  0.0 41.3 jit_solution(6943096461472695802)
XLA Ops:
  0.6 39.1 %prefill.1 = (bf16[2,2,256,512]{3,2,1,0:T(8,128)(2,1)S(1)}, bf16[2,8,256]{2,1,0:T(8,128)(2,1)S(1)}, f32[8,4,512]{2,1,0:T(4,128)S(1)}) custom-call(bf16[2,128,2048]{2,1,0:T(8,128)(2,1)} %tokens.1, bf16[256,1024]{1,0:T(8,128)(2,1)} %key_weight.1, bf16[256,1024]{1,0:T(8,128)(2,1)} %value_weight.1, bf16[2,1024]{1,0:T(2,128)(2,1)} %queries.1, f32[1,16]{1,0:T(1,128)} %bitcast.7, ...), custom_call_target="tpu_custom_call" | custom-call | tf_op jit(solution)/shard_map/prefill/pallas_call | solution.py:474
  39.7 1.6 %finish.1 = (bf16[2,256,512]{2,1,0:T(8,128)(2,1)}, bf16[2,256,512]{2,1,0:T(8,128)(2,1)}, bf16[2,8,256]{2,1,0:T(8,128)(2,1)}, f32[2,512]{1,0:T(2,128)}) custom-call(bf16[2,2,256,512]{3,2,1,0:T(8,128)(2,1)S(1)} %get-tuple-element.11.kv, bf16[2,8,256]{2,1,0:T(8,128)(2,1)S(1)} %get-tuple-element.12.bias, f32[8,4,512]{2,1,0:T(4,128)S(1)} %get-tuple-element.13.packed), custom_call_target="tpu_custom_call" | custom-call | tf_op jit(solution)/shard_map/finish/pallas_call | solution.py:519

commit v2 on v1

--- a/solution.py
+++ b/solution.py
@@ -10,9 +10,11 @@
 MESH = pl.DeviceIdType.MESH
 F32 = jnp.float32
 BF16 = jnp.bfloat16
-SUBS = 2
-MARK = 2 * SUBS
-AHEAD = 2
+VALUE_SUBS = 4
+KEY_SUBS = 4
+MARK = VALUE_SUBS + KEY_SUBS
+AHEAD = (4, 7, 10, 11)
+FILL = (0, 0, 2, 4)
 MIX_HOP = 2
 
 
@@ -33,13 +35,11 @@
     kv, bias_out, packed,
     tok, wts, acc, bias, query, offset, bias_all, bias_own, key_rows,
     ubuf, ucat, pout, pin, plow, tot_out, tot_in,
-    local_sem, ring_send, ring_recv, pair_send, pair_recv,
-    tok_send, tok_recv, bias_send, bias_recv, read_send, read_recv, mix_send, mix_recv,
+    local_sem, tok_load, sends, receives, ring_recv, last_recv, pair_recv, tok_recv,
 ):
     n, tp_count, seqs, pos, width, rows, cols, heads, head_dim, rows_h = dims
     hops = n // 2
     half_rows = rows // 2
-    sub_rows = half_rows // SUBS
     span = tp_count * pos
     kv_width = tp_count * cols
     me, tp, gr = lax.axis_index("sp"), lax.axis_index("tp"), lax.axis_index("gr")
@@ -56,22 +56,44 @@
     for h in range(1, hops + 1):
         order.extend([-h, h] if h < hops else [h])
     chunk = width // n if chunked else width
+    chunk_count = n if chunked else 1
+
+    def slot_of(step):
+        if not chunked:
+            return owner_at(step)
+        return order.index(hops if abs(step) == hops else step)
+
     my_rows = pl.ds(pl.multiple_of(tp * pos, pos), pos)
 
     key_copy = pltpu.make_async_copy(key_weight, key_rows, local_sem.at[6])
     query_copy = pltpu.make_async_copy(queries, query, local_sem.at[4])
     weight_copies = [
         pltpu.make_async_copy(
-            w.at[:, pl.ds(col_start, cols)], wts.at[part, me], local_sem.at[part]
+            w.at[:, pl.ds(col_start, cols)], wts.at[part, slot_of(0)], local_sem.at[part]
         )
         for part, w in enumerate((key_weight, value_weight))
     ]
-    tok_copy = pltpu.make_async_copy(tokens, tok.at[:, my_rows, :], local_sem.at[2])
+
+    def columns(i):
+        return slice(i * chunk, (i + 1) * chunk)
+
+    def columns_held(i):
+        if not chunked:
+            return slice(0, width)
+        return pl.ds(pl.multiple_of(owner_at(order[i]) * chunk, 128), chunk)
+
+    tok_copies = [
+        pltpu.make_async_copy(
+            tokens.at[:, :, columns_held(i)], tok.at[:, my_rows, columns(i)],
+            tok_load.at[min(i, 1)],
+        )
+        for i in range(chunk_count)
+    ]
     bias_copy = pltpu.make_async_copy(key_bias, bias_all, local_sem.at[3])
     own_bias_copy = pltpu.make_async_copy(own_bias, bias_own, local_sem.at[7])
     offset_copy = pltpu.make_async_copy(head_offset, offset, local_sem.at[5])
     for c in (
-        weight_copies[1], tok_copy, query_copy, key_copy, weight_copies[0],
+        weight_copies[1], tok_copies[0], query_copy, key_copy, *tok_copies[1:], weight_copies[0],
         bias_copy, own_bias_copy, offset_copy,
     ):
         c.start()
@@ -82,33 +104,30 @@
         pl.semaphore_signal(barrier, inc=1, device_id=target, device_id_type=MESH)
 
     def part_of(piece):
-        return 1 if piece < SUBS else 0
+        return 1 if piece < VALUE_SUBS else 0
 
     def rows_of(piece, core):
-        return pl.ds(pl.multiple_of(core * half_rows + (piece % SUBS) * sub_rows, sub_rows), sub_rows)
+        part = part_of(piece)
+        size = half_rows // (VALUE_SUBS if part == 1 else KEY_SUBS)
+        sub = piece - (0 if part == 1 else VALUE_SUBS)
+        return pl.ds(pl.multiple_of(core * half_rows + sub * size, size), size)
 
     def block_of(piece, step, core):
         if piece == MARK:
-            return ubuf.at[owner_at(step)]
-        return wts.at[part_of(piece), owner_at(step), rows_of(piece, core), :]
-
-    def ring_copy(direction, hop, piece, step):
-        block = block_of(piece, step, gr)
+            return ubuf.at[slot_of(step)]
+        return wts.at[part_of(piece), slot_of(step), rows_of(piece, core), :]
+
+    def ring_copy(direction, hop, piece):
         return pltpu.make_async_remote_copy(
-            src_ref=block, dst_ref=block,
-            send_sem=ring_send.at[direction, hop - 1, piece],
-            recv_sem=ring_recv.at[direction, hop - 1, piece],
+            src_ref=block_of(piece, step_of(direction, hop - 1), gr),
+            dst_ref=block_of(piece, step_of(direction, hop), gr),
+            send_sem=sends.at[1 if piece == MARK else 0],
+            recv_sem=(last_recv.at[piece] if hop == hops else ring_recv.at[direction, hop - 1, piece]),
             device_id={"sp": right if direction == 0 else left}, device_id_type=MESH,
         )
 
     def step_of(direction, hop):
         return -hop if direction == 0 else hop
-
-    def sent(direction, hop, piece):
-        return ring_copy(direction, hop, piece, step_of(direction, hop - 1))
-
-    def got(direction, hop, piece):
-        return ring_copy(direction, hop, piece, step_of(direction, hop))
 
     def used(direction, hop, piece):
         return hop < hops or (hop == hops and piece % 2 == direction)
@@ -117,17 +136,9 @@
         block = block_of(piece, step_of(direction, hop), core)
         return pltpu.make_async_remote_copy(
             src_ref=block, dst_ref=block,
-            send_sem=pair_send.at[direction, hop - 1, piece],
-            recv_sem=pair_recv.at[direction, hop - 1, piece],
+            send_sem=sends.at[2], recv_sem=pair_recv.at[part_of(piece), hop - 1],
             device_id={"gr": partner}, device_id_type=MESH,
         )
-
-    def tok_columns(i):
-        if not chunked:
-            return pl.ds(0, width)
-        return pl.ds(pl.multiple_of(owner_at(order[i]) * chunk, 128), chunk)
-
-    chunk_count = len(order) if chunked else 1
 
     def peer_of(k):
         return lax.rem(tp + k + 1, tp_count)
@@ -135,19 +146,19 @@
     def source_of(k):
         return lax.rem(tp + tp_count - k - 1, tp_count)
 
-    def tok_move(i, k, source):
+    def tok_move(i, s, k, source):
         place_rows = pl.ds(pl.multiple_of(source * pos, pos), pos)
-        block = tok.at[:, place_rows, tok_columns(i)]
+        block = tok.at[s, place_rows, columns(i)]
         return pltpu.make_async_remote_copy(
             src_ref=block, dst_ref=block,
-            send_sem=tok_send.at[i, k], recv_sem=tok_recv.at[i, k],
+            send_sem=sends.at[3], recv_sem=tok_recv.at[(i + 1) // 2 if chunked else 0, s],
             device_id={"tp": peer_of(k)}, device_id_type=MESH,
         )
 
     def bias_move(k, source, target):
         return pltpu.make_async_remote_copy(
             src_ref=bias_all.at[:, target], dst_ref=bias.at[source],
-            send_sem=bias_send.at[k], recv_sem=bias_recv.at[k],
+            send_sem=sends.at[4], recv_sem=receives.at[0],
             device_id={"tp": peer_of(k)}, device_id_type=MESH,
         )
 
@@ -155,49 +166,60 @@
         out, into = ((pout, pin), (tot_out, tot_in))[which]
         return pltpu.make_async_remote_copy(
             src_ref=out.at[target], dst_ref=into.at[source],
-            send_sem=read_send.at[which, k], recv_sem=read_recv.at[which, k],
+            send_sem=sends.at[5 + which], recv_sem=receives.at[1 + which],
             device_id={"tp": peer_of(k)}, device_id_type=MESH,
         )
-
-    sent_list = []
 
     def launch(c):
         c.start()
-        sent_list.append(c)
+
+    def counted(ref, sem):
+        return pltpu.make_async_copy(ref, ref, sem)
 
     issued = [0]
 
+    def load_tokens(i):
+        if i == 0:
+            tok_copies[0].wait()
+        else:
+            counted(tok.at[:, my_rows, chunk:], tok_load.at[1]).wait()
+
     def send_tokens(upto):
-        while issued[0] < min(upto, chunk_count):
+        while issued[0] < min(upto, chunk_count * seqs):
+            i, s = divmod(issued[0], seqs)
+            if s == 0 and i < 2:
+                load_tokens(i)
             for k in range(tp_count - 1):
-                launch(tok_move(issued[0], k, tp))
+                launch(tok_move(i, s, k, tp))
             issued[0] += 1
 
     def open_ring(piece):
         for direction in range(2):
             if used(direction, 1, piece):
-                launch(sent(direction, 1, piece))
+                launch(ring_copy(direction, 1, piece))
 
     def pass_on(hop, pieces):
         for piece in pieces:
             for direction in range(2):
                 if not used(direction, hop, piece):
                     continue
-                got(direction, hop, piece).wait_recv()
+                ring_copy(direction, hop, piece).wait_recv()
                 if hop < hops and used(direction, hop + 1, piece):
-                    launch(sent(direction, hop + 1, piece))
+                    launch(ring_copy(direction, hop + 1, piece))
                 if piece != MARK:
                     launch(pair_copy(direction, hop, piece, gr))
 
-    value_pieces = list(range(SUBS))
-    key_pieces = list(range(SUBS, 2 * SUBS))
+    value_pieces = list(range(VALUE_SUBS))
+    key_pieces = list(range(VALUE_SUBS, MARK))
     first_pass = value_pieces[:1] + [MARK] + value_pieces[1:]
 
-    pl.semaphore_wait(barrier, 3 + len(tp_peers))
-    weight_copies[1].wait()
+    with jax.named_scope("barrier"):
+        pl.semaphore_wait(barrier, 3 + len(tp_peers))
+    with jax.named_scope("weights"):
+        weight_copies[1].wait()
     open_ring(value_pieces[0])
-    tok_copy.wait()
-    send_tokens(AHEAD)
+    with jax.named_scope("tokens"):
+        send_tokens(AHEAD[0])
 
     query_copy.wait()
     key_copy.wait()
@@ -210,7 +232,7 @@
     q_rows = jnp.concatenate(
         [jnp.where(mine, q[s : s + 1], 0.0) for s in range(seqs)], axis=0
     ).astype(BF16)
-    ubuf[me] = lax.dot_general(
+    ubuf[slot_of(0)] = lax.dot_general(
         q_rows, key_rows[...], (((1,), (1,)), ((), ())), preferred_element_type=F32
     ).astype(BF16)
     for piece in value_pieces[1:]:
@@ -223,12 +245,80 @@
     own_bias_copy.wait()
     offset_copy.wait()
 
-    for hop in range(1, hops + 1):
-        pass_on(hop, first_pass)
-        send_tokens(AHEAD + hop)
-        if hop == max(hops - 1, 1):
-            for piece in key_pieces:
+    key_queue = [(0, piece) for piece in key_pieces]
+    key_queue += [(hop, piece) for hop in range(1, hops + 1) for piece in key_pieces]
+
+    def next_key():
+        hop, piece = key_queue.pop(0)
+        with jax.named_scope(f"key{hop}_{piece}"):
+            if hop == 0:
                 open_ring(piece)
+            else:
+                pass_on(hop, [piece])
+
+    seen = set()
+
+    def pair_ready(part, hop):
+        if hop == 0 or ("pair", part, hop) in seen:
+            return
+        seen.add(("pair", part, hop))
+        held = wts.at[part, slot_of(hop)]
+        if hop == hops:
+            held = held.at[pl.ds(0, half_rows), :]
+        counted(held, pair_recv.at[part, hop - 1]).wait()
+
+    def tokens_ready(hop, s):
+        if ("tok", hop, s) in seen or tp_count == 1:
+            return
+        seen.add(("tok", hop, s))
+        first, end = slots_of_hop(hop) if chunked else (0, 1)
+        counted(
+            tok.at[s, pl.ds(0, (tp_count - 1) * pos), slice(first * chunk, end * chunk)],
+            tok_recv.at[hop, s],
+        ).wait()
+
+    def slots_of_hop(hop):
+        if hop == 0:
+            return 0, 1
+        first = 1 + 2 * (hop - 1)
+        return first, min(first + 2, n)
+
+    def multiply(part, hop):
+        if not chunked or ("done", part, hop) in seen:
+            return
+        seen.add(("done", part, hop))
+        first, end = slots_of_hop(hop)
+        with jax.named_scope(f"multiply{part}_{hop}"):
+            pair_ready(part, hop)
+            w = wts[part, first:end].reshape((end - first) * rows, cols)
+            for s in range(seqs):
+                tokens_ready(hop, s)
+                y = jnp.dot(
+                    tok[s, :, first * chunk : end * chunk], w, preferred_element_type=F32
+                )
+                if hop > 0:
+                    y = acc[part, s] + y
+                if hop < hops:
+                    acc[part, s] = y
+                else:
+                    kv[part, s] = y.astype(BF16)
+
+    for hop in range(1, hops):
+        with jax.named_scope(f"value{hop}"):
+            pass_on(hop, first_pass)
+        send_tokens(AHEAD[min(hop, len(AHEAD) - 1)])
+        for _ in range(FILL[min(hop, len(FILL) - 1)]):
+            if key_queue[0][0] < hop:
+                next_key()
+        if hop == 2:
+            multiply(1, 0)
+            multiply(0, 0)
+        if hop == 3:
+            multiply(1, 1)
+    while key_queue[0][0] == 0:
+        next_key()
+    with jax.named_scope("marks"):
+        pass_on(hops, [MARK])
 
     for owner in range(n):
         ucat[:, owner * rows : (owner + 1) * rows] = ubuf[owner]
@@ -278,7 +368,6 @@
         )
         for s in range(seqs)
     ]
-    lows = []
     for t in range(tp_count):
         at = slice(t * rows_h, (t + 1) * rows_h)
         tot_out[t] = jnp.concatenate(
@@ -294,77 +383,24 @@
             launch(read_move(k, which, tp, peer_of(k)))
     pin[tp] = pout[tp]
     tot_in[tp] = tot_out[tp]
-    send_tokens(chunk_count)
-
-    def pair_ready(hop, pieces):
-        for direction in range(2):
-            for piece in pieces:
-                if used(direction, hop, piece):
-                    pair_copy(direction, hop, piece, partner).wait_recv()
-
-    for hop in range(1, hops + 1):
-        pair_ready(hop, value_pieces)
-
-    def tokens_ready(i):
-        for k in range(tp_count - 1):
-            tok_move(i, k, source_of(k)).wait_recv()
-
-    def multiply(i):
-        owner = owner_at(order[i])
-        for part in range(2):
-            w = wts[part, owner]
-
-            def body(s, carry):
-                x = tok[s, :, tok_columns(i)]
-                y = jnp.dot(x, w, preferred_element_type=F32)
-                if i > 0:
-                    y = acc[part, s] + y
-                acc[part, s] = y
-                return carry
-
-            lax.fori_loop(0, seqs, body, 0)
-
-    def close(i, source):
-        owner = owner_at(order[i])
-        where = pl.ds(pl.multiple_of(source * pos, pos), pos)
-        for part in range(2):
-            for s in range(seqs):
-                y = jnp.dot(
-                    tok[s, where, tok_columns(i)], wts[part, owner], preferred_element_type=F32
-                )
-                kv[part, s, where, :] = (acc[part, s, where, :] + y).astype(BF16)
-
-    def steps_of_hop(hop):
-        if hop == 0:
-            return [0]
-        first = 1 + 2 * (hop - 1)
-        return [first, first + 1] if hop < hops else [first]
-
-    def compute_hop(hop):
-        if hop > 0:
-            pair_ready(hop, key_pieces)
-        if chunked:
-            for i in steps_of_hop(hop):
-                if i < len(order) - 1:
-                    tokens_ready(i)
-                    multiply(i)
-                else:
-                    close(i, tp)
-                    tokens_ready(i)
-                    for p in tp_peers:
-                        close(i, p)
+    send_tokens(chunk_count * seqs)
+    with jax.named_scope(f"value{hops}"):
+        pass_on(hops, value_pieces)
 
     def mix_move(k, source):
         return pltpu.make_async_remote_copy(
             src_ref=packed.at[source], dst_ref=packed.at[source],
-            send_sem=mix_send.at[k - 1], recv_sem=mix_recv.at[k - 1],
+            send_sem=sends.at[7], recv_sem=receives.at[3],
             device_id={"sp": lax.rem(me + k, n)}, device_id_type=MESH,
         )
 
     def mix():
-        for k in range(tp_count - 1):
-            for which in range(2):
-                read_move(k, which, source_of(k), tp).wait_recv()
+        with jax.named_scope("await_products"):
+            if tp_count > 1:
+                counted(pin.at[pl.ds(0, tp_count - 1)], receives.at[1]).wait()
+                counted(tot_in.at[pl.ds(0, tp_count - 1)], receives.at[2]).wait()
+            for hop in range(1, hops + 1):
+                pair_ready(1, hop)
         count = seqs * rows_h
         given = jnp.concatenate([pin[t] for t in range(tp_count)] + [plow[tp]], axis=0)
         product = jnp.dot(
@@ -392,14 +428,21 @@
             launch(mix_move(k, me))
 
     for hop in range(1, hops + 1):
-        pass_on(hop, key_pieces)
+        while key_queue and key_queue[0][0] <= hop:
+            next_key()
         if hop == min(MIX_HOP, hops):
             mix()
-        compute_hop(hop - 1)
-    compute_hop(hops)
+        for step in range(min(hop + 1, hops)):
+            multiply(1, step)
+            multiply(0, step)
+    multiply(1, hops)
+    multiply(0, hops)
 
     if not chunked:
-        tokens_ready(0)
+        for s in range(seqs):
+            tokens_ready(0, s)
+        for hop in range(1, hops + 1):
+            pair_ready(0, hop)
         tile = pos
         for part in range(2):
             w = wts[part].reshape(width, cols)
@@ -413,15 +456,24 @@
 
             lax.fori_loop(0, seqs * (span // tile), body, 0)
 
-    for k in range(tp_count - 1):
-        bias_move(k, source_of(k), tp).wait_recv()
+    if tp_count > 1:
+        counted(bias.at[pl.ds(0, tp_count - 1)], receives.at[0]).wait()
     bias[tp] = bias_all[:, tp]
     for s in range(seqs):
         bias_out[s] = jnp.concatenate([bias[t, s] for t in range(tp_count)], axis=1)
-    for k in range(1, n):
-        mix_move(k, lax.rem(me + n - k, n)).wait_recv()
-    for c in sent_list:
-        c.wait_send()
+    with jax.named_scope("await_mix"):
+        counted(packed.at[pl.ds(0, n - 1)], receives.at[3]).wait()
+    with jax.named_scope("drain"):
+        counted(wts.at[0, pl.ds(0, n - 1)], sends.at[0]).wait()
+        counted(ubuf.at[pl.ds(0, n - 1)], sends.at[1]).wait()
+        counted(wts.at[0, pl.ds(0, n - 1)], sends.at[2]).wait()
+        if tp_count > 1:
+            others = pl.ds(0, tp_count - 1)
+            counted(tok.at[:, pl.ds(0, (tp_count - 1) * pos), :], sends.at[3]).wait()
+            counted(bias.at[others], sends.at[4]).wait()
+            counted(pin.at[others], sends.at[5]).wait()
+            counted(tot_in.at[others], sends.at[6]).wait()
+        counted(packed.at[pl.ds(0, n - 1)], sends.at[7]).wait()
 
 
 def finish(n, head_dim, kv, bias, packed, key_out, value_out, bias_out, reading_out, sems):
@@ -468,8 +520,7 @@
     own_bias = jnp.pad(bias_rows, ((0, 0), (0, 0), (0, rows_h - heads), (0, 0)))
     own_bias = own_bias.reshape(seqs, group, pos)
     dims = (n, tp_count, seqs, pos, width, rows, cols, heads, head_dim, rows_h)
-    peers = max(tp_count - 1, 1)
-    chunks = n if (width // n) % 128 == 0 else 1
+    groups = hops + 1 if (width // n) % 128 == 0 else 1
     dma = pltpu.SemaphoreType.DMA
     kv, bias_held, packed = pl.pallas_call(
         functools.partial(kernel, dims),
@@ -498,18 +549,13 @@
             pltpu.VMEM((tp_count, seqs * rows_h, 128), F32),
             pltpu.VMEM((tp_count, seqs * rows_h, 128), F32),
             dma((8,)),
-            dma((2, hops, MARK + 1)),
-            dma((2, hops, MARK + 1)),
-            dma((2, hops, MARK + 1)),
-            dma((2, hops, MARK + 1)),
-            dma((chunks, peers)),
-            dma((chunks, peers)),
-            dma((peers,)),
-            dma((peers,)),
-            dma((2, peers)),
-            dma((2, peers)),
-            dma((n - 1,)),
-            dma((n - 1,)),
+            dma((2,)),
+            dma((8,)),
+            dma((4,)),
+            dma((2, hops - 1, MARK + 1)),
+            dma((MARK + 1,)),
+            dma((2, hops)),
+            dma((groups, seqs)),
         ],
         compiler_params=pltpu.CompilerParams(
             collective_id=0, has_side_effects=True, vmem_limit_bytes=36 * 2**20

time: 41.5 us -> 36.5 us (0.88)
  Pallas kernels: 40.7 us -> 35.6 us
    pallas_call x1, Pallas kernels: 39.1 us -> 34 us  [per_device(): pl.pallas_call(functools.partial(kernel, dims), out_shape=(jax.ShapeDtype...]
where the time goes in v2:
time: 36.5 us; the launch traced here: 36.2 us
  Pallas kernels  35.6 us (98%)
  between operations  0.64 us (2%)
    pallas_call x1, Pallas kernels, per_device(): pl.pallas_call(functools.partial(kernel, dims), out_shape=(jax.ShapeDtype...  34 us
    pallas_call x1, Pallas kernels, per_device(): pl.pallas_call(functools.partial(finish, n, head_dim), out_shape=(jax.Sha...  1.6 us

profile of v2, /device:TPU:0, one launch (start us, length us, event | category | flops | bytes accessed | tf_op | source)
XLA Modules:
  0.0 36.2 jit_solution(5188657612707886587)
XLA Ops:
  0.6 34.0 %prefill.1 = (bf16[2,2,256,512]{3,2,1,0:T(8,128)(2,1)S(1)}, bf16[2,8,256]{2,1,0:T(8,128)(2,1)S(1)}, f32[8,4,512]{2,1,0:T(4,128)S(1)}) custom-call(bf16[2,128,2048]{2,1,0:T(8,128)(2,1)} %tokens.1, bf16[256,1024]{1,0:T(8,128)(2,1)} %key_weight.1, bf16[256,1024]{1,0:T(8,128)(2,1)} %value_weight.1, bf16[2,1024]{1,0:T(2,128)(2,1)} %queries.1, f32[1,16]{1,0:T(1,128)} %bitcast.7, ...), custom_call_target="tpu_custom_call" | custom-call | tf_op jit(solution)/shard_map/prefill/pallas_call | solution.py:525
  34.6 1.6 %finish.1 = (bf16[2,256,512]{2,1,0:T(8,128)(2,1)}, bf16[2,256,512]{2,1,0:T(8,128)(2,1)}, bf16[2,8,256]{2,1,0:T(8,128)(2,1)}, f32[2,512]{1,0:T(2,128)}) custom-call(bf16[2,2,256,512]{3,2,1,0:T(8,128)(2,1)S(1)} %get-tuple-element.11.kv, bf16[2,8,256]{2,1,0:T(8,128)(2,1)S(1)} %get-tuple-element.12.bias, f32[8,4,512]{2,1,0:T(4,128)S(1)} %get-tuple-element.13.packed), custom_call_target="tpu_custom_call" | custom-call | tf_op jit(solution)/shard_map/finish/pallas_call | solution.py:565

commit v3 on v2

--- a/solution.py
+++ b/solution.py
@@ -10,12 +10,43 @@
 MESH = pl.DeviceIdType.MESH
 F32 = jnp.float32
 BF16 = jnp.bfloat16
-VALUE_SUBS = 4
-KEY_SUBS = 4
+VALUE_SUBS = 2
+KEY_SUBS = 2
 MARK = VALUE_SUBS + KEY_SUBS
-AHEAD = (4, 7, 10, 11)
-FILL = (0, 0, 2, 4)
-MIX_HOP = 2
+OPEN, PASS, TOKENS, MULTIPLY, PROJECT, READ, MIX = range(7)
+
+
+def plan(hops, seqs):
+    if hops == 4 and seqs == 2:
+        return TUNED
+    value, key = range(VALUE_SUBS), range(VALUE_SUBS, MARK)
+    first = [0, MARK, *value[1:]]
+    steps = [(OPEN, 0), (TOKENS, 4), (PROJECT,), *((OPEN, p) for p in first[1:])]
+    for hop in range(1, hops):
+        steps += [(PASS, hop, p) for p in first] + [(TOKENS, 4 + 2 * hop)]
+    steps += [(OPEN, p) for p in key]
+    steps += [(PASS, hops, p) for p in first] + [(READ,), (TOKENS, 4 * hops * seqs)]
+    for hop in range(1, hops + 1):
+        steps += [(PASS, hop, p) for p in key]
+        if hop == min(2, hops):
+            steps.append((MIX,))
+        for h in range(hop + 1) if hop == 1 else [hop]:
+            steps += [(MULTIPLY, part, h, s) for part in (1, 0) for s in range(seqs)]
+    return steps
+
+
+TUNED = (
+    (OPEN, 0), (TOKENS, 10), (PROJECT,), (OPEN, MARK), (OPEN, 1), (PASS, 1, 0), (PASS, 1, MARK),
+    (OPEN, 2), (PASS, 1, 1), (MULTIPLY, 0, 0, 0), (MULTIPLY, 1, 0, 1), (PASS, 2, MARK), (OPEN, 3),
+    (PASS, 2, 0), (PASS, 3, MARK), (MULTIPLY, 1, 0, 0), (MULTIPLY, 0, 0, 1), (PASS, 2, 1),
+    (PASS, 1, 2), (PASS, 1, 3), (MULTIPLY, 1, 1, 0), (PASS, 4, MARK), (READ,), (TOKENS, 15),
+    (PASS, 3, 0), (MULTIPLY, 0, 1, 1), (TOKENS, 16), (PASS, 3, 1), (MULTIPLY, 1, 2, 1),
+    (MULTIPLY, 0, 1, 0), (PASS, 2, 2), (MULTIPLY, 1, 1, 1), (PASS, 2, 3), (PASS, 4, 1),
+    (PASS, 4, 0), (MIX,), (PASS, 3, 2), (PASS, 3, 3), (MULTIPLY, 0, 2, 0), (MULTIPLY, 1, 3, 0),
+    (MULTIPLY, 0, 3, 0), (MULTIPLY, 1, 2, 0), (MULTIPLY, 1, 3, 1), (MULTIPLY, 1, 4, 0),
+    (MULTIPLY, 0, 2, 1), (MULTIPLY, 0, 3, 1), (PASS, 4, 3), (PASS, 4, 2), (MULTIPLY, 1, 4, 1),
+    (MULTIPLY, 0, 4, 0), (MULTIPLY, 0, 4, 1),
+)
 
 
 def ring_place(index, length):
@@ -42,6 +73,7 @@
     half_rows = rows // 2
     span = tp_count * pos
     kv_width = tp_count * cols
+    group = tp_count * rows_h
     me, tp, gr = lax.axis_index("sp"), lax.axis_index("tp"), lax.axis_index("gr")
     place = ring_place(me, n)
 
@@ -198,65 +230,107 @@
             if used(direction, 1, piece):
                 launch(ring_copy(direction, 1, piece))
 
-    def pass_on(hop, pieces):
-        for piece in pieces:
-            for direction in range(2):
-                if not used(direction, hop, piece):
-                    continue
-                ring_copy(direction, hop, piece).wait_recv()
-                if hop < hops and used(direction, hop + 1, piece):
-                    launch(ring_copy(direction, hop + 1, piece))
-                if piece != MARK:
-                    launch(pair_copy(direction, hop, piece, gr))
-
-    value_pieces = list(range(VALUE_SUBS))
-    key_pieces = list(range(VALUE_SUBS, MARK))
-    first_pass = value_pieces[:1] + [MARK] + value_pieces[1:]
-
-    with jax.named_scope("barrier"):
-        pl.semaphore_wait(barrier, 3 + len(tp_peers))
-    with jax.named_scope("weights"):
-        weight_copies[1].wait()
-    open_ring(value_pieces[0])
-    with jax.named_scope("tokens"):
-        send_tokens(AHEAD[0])
-
-    query_copy.wait()
-    key_copy.wait()
-    group = tp_count * rows_h
-    row = lax.broadcasted_iota(jnp.int32, (group, kv_width), 0)
-    col_head = lax.broadcasted_iota(jnp.int32, (group, kv_width), 1) // head_dim
-    inner = lax.rem(row, rows_h)
-    mine = (row // rows_h * heads + inner == col_head) & (inner < heads)
-    q = query[...].astype(F32)
-    q_rows = jnp.concatenate(
-        [jnp.where(mine, q[s : s + 1], 0.0) for s in range(seqs)], axis=0
-    ).astype(BF16)
-    ubuf[slot_of(0)] = lax.dot_general(
-        q_rows, key_rows[...], (((1,), (1,)), ((), ())), preferred_element_type=F32
-    ).astype(BF16)
-    for piece in value_pieces[1:]:
-        open_ring(piece)
-    open_ring(MARK)
-    bias_copy.wait()
-    for k in range(tp_count - 1):
-        launch(bias_move(k, tp, peer_of(k)))
-    weight_copies[0].wait()
-    own_bias_copy.wait()
-    offset_copy.wait()
-
-    key_queue = [(0, piece) for piece in key_pieces]
-    key_queue += [(hop, piece) for hop in range(1, hops + 1) for piece in key_pieces]
-
-    def next_key():
-        hop, piece = key_queue.pop(0)
-        with jax.named_scope(f"key{hop}_{piece}"):
-            if hop == 0:
-                open_ring(piece)
-            else:
-                pass_on(hop, [piece])
+    def pass_on(hop, piece):
+        for direction in range(2):
+            if not used(direction, hop, piece):
+                continue
+            ring_copy(direction, hop, piece).wait_recv()
+            if hop < hops and used(direction, hop + 1, piece):
+                launch(ring_copy(direction, hop + 1, piece))
+            if piece != MARK:
+                launch(pair_copy(direction, hop, piece, gr))
+
+    def project():
+        query_copy.wait()
+        key_copy.wait()
+        row = lax.broadcasted_iota(jnp.int32, (group, kv_width), 0)
+        col_head = lax.broadcasted_iota(jnp.int32, (group, kv_width), 1) // head_dim
+        inner = lax.rem(row, rows_h)
+        mine = (row // rows_h * heads + inner == col_head) & (inner < heads)
+        q = query[...].astype(F32)
+        q_rows = jnp.concatenate(
+            [jnp.where(mine, q[s : s + 1], 0.0) for s in range(seqs)], axis=0
+        ).astype(BF16)
+        ubuf[slot_of(0)] = lax.dot_general(
+            q_rows, key_rows[...], (((1,), (1,)), ((), ())), preferred_element_type=F32
+        ).astype(BF16)
+        bias_copy.wait()
+        for k in range(tp_count - 1):
+            launch(bias_move(k, tp, peer_of(k)))
+
+    def read():
+        own_bias_copy.wait()
+        offset_copy.wait()
+        for owner in range(n):
+            ucat[:, owner * rows : (owner + 1) * rows] = ubuf[owner]
+        total_heads = offset.shape[1]
+        pick_row = lax.broadcasted_iota(jnp.int32, (group, total_heads), 0)
+        pick_inner = lax.rem(pick_row, rows_h)
+        pick = (
+            lax.broadcasted_iota(jnp.int32, (group, total_heads), 1)
+            == pick_row // rows_h * heads + pick_inner
+        ) & (pick_inner < heads)
+        offset_col = jnp.sum(jnp.where(pick, offset[...], 0.0), axis=1, keepdims=True)
+        logits = []
+        for s in range(seqs):
+            logits.append(
+                lax.dot_general(
+                    ucat[s * group : (s + 1) * group, :], tok[s, my_rows, :],
+                    (((1,), (1,)), ((), ())), preferred_element_type=F32,
+                )
+                * (head_dim**-0.5)
+                + offset_col
+                + bias_own[s].astype(F32)
+            )
+        logits = jnp.concatenate(logits, axis=0)
+        soft = jnp.log1p(jnp.exp(-jnp.abs(logits)))
+        fading = -jnp.maximum(logits, 0.0) - soft
+        taking = jnp.minimum(logits, 0.0) - soft
+        high = fading.astype(BF16)
+        rest = fading - high.astype(F32)
+        mid = rest.astype(BF16)
+        low = (rest - mid.astype(F32)).astype(BF16)
+        later = (
+            lax.broadcasted_iota(jnp.int32, (pos, pos), 0)
+            > lax.broadcasted_iota(jnp.int32, (pos, pos), 1)
+        ).astype(F32).astype(BF16)
+        sums = jnp.dot(
+            jnp.concatenate([high, mid, low], axis=0), later, preferred_element_type=F32
+        )
+        m = seqs * group
+        within = sums[:m] + sums[m : 2 * m] + sums[2 * m :]
+        weights = jnp.exp(taking + within).astype(BF16)
+        totals = jnp.sum(fading, axis=1, keepdims=True)
+        spread = jnp.broadcast_to(totals, (m, 128))
+        weighted = [
+            jnp.dot(
+                weights[s * group : (s + 1) * group], tok[s, my_rows, :],
+                preferred_element_type=F32,
+            )
+            for s in range(seqs)
+        ]
+        for t in range(tp_count):
+            at = slice(t * rows_h, (t + 1) * rows_h)
+            tot_out[t] = jnp.concatenate(
+                [spread[s * group + t * rows_h : s * group + (t + 1) * rows_h] for s in range(seqs)],
+                axis=0,
+            )
+            whole = jnp.concatenate([weighted[s][at] for s in range(seqs)], axis=0)
+            upper = whole.astype(BF16)
+            pout[t] = upper
+            plow[t] = (whole - upper.astype(F32)).astype(BF16)
+        for k in range(tp_count - 1):
+            for which in range(2):
+                launch(read_move(k, which, tp, peer_of(k)))
+        pin[tp] = pout[tp]
+        tot_in[tp] = tot_out[tp]
 
     seen = set()
+
+    def weights_here(part):
+        if ("weights", part) not in seen:
+            seen.add(("weights", part))
+            weight_copies[part].wait()
 
     def pair_ready(part, hop):
         if hop == 0 or ("pair", part, hop) in seen:
@@ -283,109 +357,26 @@
         first = 1 + 2 * (hop - 1)
         return first, min(first + 2, n)
 
-    def multiply(part, hop):
-        if not chunked or ("done", part, hop) in seen:
+    def multiply(part, hop, s):
+        if not chunked:
             return
-        seen.add(("done", part, hop))
         first, end = slots_of_hop(hop)
-        with jax.named_scope(f"multiply{part}_{hop}"):
+        with jax.named_scope(f"multiply{part}_{hop}_{s}"):
+            if hop == 0:
+                weights_here(part)
             pair_ready(part, hop)
-            w = wts[part, first:end].reshape((end - first) * rows, cols)
-            for s in range(seqs):
-                tokens_ready(hop, s)
-                y = jnp.dot(
-                    tok[s, :, first * chunk : end * chunk], w, preferred_element_type=F32
-                )
-                if hop > 0:
-                    y = acc[part, s] + y
-                if hop < hops:
-                    acc[part, s] = y
-                else:
-                    kv[part, s] = y.astype(BF16)
-
-    for hop in range(1, hops):
-        with jax.named_scope(f"value{hop}"):
-            pass_on(hop, first_pass)
-        send_tokens(AHEAD[min(hop, len(AHEAD) - 1)])
-        for _ in range(FILL[min(hop, len(FILL) - 1)]):
-            if key_queue[0][0] < hop:
-                next_key()
-        if hop == 2:
-            multiply(1, 0)
-            multiply(0, 0)
-        if hop == 3:
-            multiply(1, 1)
-    while key_queue[0][0] == 0:
-        next_key()
-    with jax.named_scope("marks"):
-        pass_on(hops, [MARK])
-
-    for owner in range(n):
-        ucat[:, owner * rows : (owner + 1) * rows] = ubuf[owner]
-    total_heads = offset.shape[1]
-    pick_row = lax.broadcasted_iota(jnp.int32, (group, total_heads), 0)
-    pick_inner = lax.rem(pick_row, rows_h)
-    pick = (
-        lax.broadcasted_iota(jnp.int32, (group, total_heads), 1)
-        == pick_row // rows_h * heads + pick_inner
-    ) & (pick_inner < heads)
-    offset_col = jnp.sum(jnp.where(pick, offset[...], 0.0), axis=1, keepdims=True)
-    logits = []
-    for s in range(seqs):
-        logits.append(
-            lax.dot_general(
-                ucat[s * group : (s + 1) * group, :], tok[s, my_rows, :],
-                (((1,), (1,)), ((), ())), preferred_element_type=F32,
+            tokens_ready(hop, s)
+            y = jnp.dot(
+                tok[s, :, first * chunk : end * chunk],
+                wts[part, first:end].reshape((end - first) * rows, cols),
+                preferred_element_type=F32,
             )
-            * (head_dim**-0.5)
-            + offset_col
-            + bias_own[s].astype(F32)
-        )
-    logits = jnp.concatenate(logits, axis=0)
-    soft = jnp.log1p(jnp.exp(-jnp.abs(logits)))
-    fading = -jnp.maximum(logits, 0.0) - soft
-    taking = jnp.minimum(logits, 0.0) - soft
-    high = fading.astype(BF16)
-    rest = fading - high.astype(F32)
-    mid = rest.astype(BF16)
-    low = (rest - mid.astype(F32)).astype(BF16)
-    later = (
-        lax.broadcasted_iota(jnp.int32, (pos, pos), 0)
-        > lax.broadcasted_iota(jnp.int32, (pos, pos), 1)
-    ).astype(F32).astype(BF16)
-    sums = jnp.dot(
-        jnp.concatenate([high, mid, low], axis=0), later, preferred_element_type=F32
-    )
-    m = seqs * group
-    within = sums[:m] + sums[m : 2 * m] + sums[2 * m :]
-    weights = jnp.exp(taking + within).astype(BF16)
-    totals = jnp.sum(fading, axis=1, keepdims=True)
-    spread = jnp.broadcast_to(totals, (m, 128))
-    weighted = [
-        jnp.dot(
-            weights[s * group : (s + 1) * group], tok[s, my_rows, :],
-            preferred_element_type=F32,
-        )
-        for s in range(seqs)
-    ]
-    for t in range(tp_count):
-        at = slice(t * rows_h, (t + 1) * rows_h)
-        tot_out[t] = jnp.concatenate(
-            [spread[s * group + t * rows_h : s * group + (t + 1) * rows_h] for s in range(seqs)],
-            axis=0,
-        )
-        whole = jnp.concatenate([weighted[s][at] for s in range(seqs)], axis=0)
-        upper = whole.astype(BF16)
-        pout[t] = upper
-        plow[t] = (whole - upper.astype(F32)).astype(BF16)
-    for k in range(tp_count - 1):
-        for which in range(2):
-            launch(read_move(k, which, tp, peer_of(k)))
-    pin[tp] = pout[tp]
-    tot_in[tp] = tot_out[tp]
-    send_tokens(chunk_count * seqs)
-    with jax.named_scope(f"value{hops}"):
-        pass_on(hops, value_pieces)
+            if hop > 0:
+                y = acc[part, s] + y
+            if hop < hops:
+                acc[part, s] = y
+            else:
+                kv[part, s] = y.astype(BF16)
 
     def mix_move(k, source):
         return pltpu.make_async_remote_copy(
@@ -427,16 +418,29 @@
         for k in range(1, n):
             launch(mix_move(k, me))
 
-    for hop in range(1, hops + 1):
-        while key_queue and key_queue[0][0] <= hop:
-            next_key()
-        if hop == min(MIX_HOP, hops):
-            mix()
-        for step in range(min(hop + 1, hops)):
-            multiply(1, step)
-            multiply(0, step)
-    multiply(1, hops)
-    multiply(0, hops)
+    with jax.named_scope("barrier"):
+        pl.semaphore_wait(barrier, 3 + len(tp_peers))
+    for kind, *what in plan(hops, seqs):
+        if kind == OPEN:
+            if what[0] != MARK:
+                weights_here(part_of(what[0]))
+            open_ring(what[0])
+        elif kind == PASS:
+            with jax.named_scope(f"pass{what[0]}_{what[1]}"):
+                pass_on(*what)
+        elif kind == TOKENS:
+            send_tokens(what[0])
+        elif kind == MULTIPLY:
+            multiply(*what)
+        elif kind == PROJECT:
+            with jax.named_scope("project"):
+                project()
+        elif kind == READ:
+            with jax.named_scope("read"):
+                read()
+        elif kind == MIX:
+            with jax.named_scope("mix"):
+                mix()
 
     if not chunked:
         for s in range(seqs):

time: 36.5 us -> 34.3 us (0.940)
  Pallas kernels: 35.6 us -> 33.3 us
    pallas_call x1, Pallas kernels: 34 us -> 31.7 us  [per_device(): pl.pallas_call(functools.partial(kernel, dims), out_shape=(jax.ShapeDtype...]
where the time goes in v3:
time: 34.3 us; the launch traced here: 34 us
  Pallas kernels  33.3 us (97%)
  between operations  0.64 us (2%)
    pallas_call x1, Pallas kernels, per_device(): pl.pallas_call(functools.partial(kernel, dims), out_shape=(jax.ShapeDtype...  31.7 us
    pallas_call x1, Pallas kernels, per_device(): pl.pallas_call(functools.partial(finish, n, head_dim), out_shape=(jax.Sha...  1.6 us

profile of v3, /device:TPU:0, one launch (start us, length us, event | category | flops | bytes accessed | tf_op | source)
XLA Modules:
  0.0 34.0 jit_solution(18135606071930653140)
XLA Ops:
  0.6 31.7 %prefill.1 = (bf16[2,2,256,512]{3,2,1,0:T(8,128)(2,1)S(1)}, bf16[2,8,256]{2,1,0:T(8,128)(2,1)S(1)}, f32[8,4,512]{2,1,0:T(4,128)S(1)}) custom-call(bf16[2,128,2048]{2,1,0:T(8,128)(2,1)} %tokens.1, bf16[256,1024]{1,0:T(8,128)(2,1)} %key_weight.1, bf16[256,1024]{1,0:T(8,128)(2,1)} %value_weight.1, bf16[2,1024]{1,0:T(2,128)(2,1)} %queries.1, f32[1,16]{1,0:T(1,128)} %bitcast.7, ...), custom_call_target="tpu_custom_call" | custom-call | tf_op jit(solution)/shard_map/prefill/pallas_call | solution.py:529
  32.4 1.6 %finish.1 = (bf16[2,256,512]{2,1,0:T(8,128)(2,1)}, bf16[2,256,512]{2,1,0:T(8,128)(2,1)}, bf16[2,8,256]{2,1,0:T(8,128)(2,1)}, f32[2,512]{1,0:T(2,128)}) custom-call(bf16[2,2,256,512]{3,2,1,0:T(8,128)(2,1)S(1)} %get-tuple-element.11.kv, bf16[2,8,256]{2,1,0:T(8,128)(2,1)S(1)} %get-tuple-element.12.bias, f32[8,4,512]{2,1,0:T(4,128)S(1)} %get-tuple-element.13.packed), custom_call_target="tpu_custom_call" | custom-call | tf_op jit(solution)/shard_map/finish/pallas_call | solution.py:569

commit v4 on v3

--- a/solution.py
+++ b/solution.py
@@ -11,8 +11,9 @@
 F32 = jnp.float32
 BF16 = jnp.bfloat16
 VALUE_SUBS = 2
-KEY_SUBS = 2
+KEY_SUBS = 4
 MARK = VALUE_SUBS + KEY_SUBS
+EARLY_HOPS = 2
 OPEN, PASS, TOKENS, MULTIPLY, PROJECT, READ, MIX = range(7)
 
 
@@ -36,16 +37,18 @@
 
 
 TUNED = (
-    (OPEN, 0), (TOKENS, 10), (PROJECT,), (OPEN, MARK), (OPEN, 1), (PASS, 1, 0), (PASS, 1, MARK),
-    (OPEN, 2), (PASS, 1, 1), (MULTIPLY, 0, 0, 0), (MULTIPLY, 1, 0, 1), (PASS, 2, MARK), (OPEN, 3),
-    (PASS, 2, 0), (PASS, 3, MARK), (MULTIPLY, 1, 0, 0), (MULTIPLY, 0, 0, 1), (PASS, 2, 1),
-    (PASS, 1, 2), (PASS, 1, 3), (MULTIPLY, 1, 1, 0), (PASS, 4, MARK), (READ,), (TOKENS, 15),
-    (PASS, 3, 0), (MULTIPLY, 0, 1, 1), (TOKENS, 16), (PASS, 3, 1), (MULTIPLY, 1, 2, 1),
-    (MULTIPLY, 0, 1, 0), (PASS, 2, 2), (MULTIPLY, 1, 1, 1), (PASS, 2, 3), (PASS, 4, 1),
-    (PASS, 4, 0), (MIX,), (PASS, 3, 2), (PASS, 3, 3), (MULTIPLY, 0, 2, 0), (MULTIPLY, 1, 3, 0),
-    (MULTIPLY, 0, 3, 0), (MULTIPLY, 1, 2, 0), (MULTIPLY, 1, 3, 1), (MULTIPLY, 1, 4, 0),
-    (MULTIPLY, 0, 2, 1), (MULTIPLY, 0, 3, 1), (PASS, 4, 3), (PASS, 4, 2), (MULTIPLY, 1, 4, 1),
-    (MULTIPLY, 0, 4, 0), (MULTIPLY, 0, 4, 1),
+    (OPEN, 0), (TOKENS, 6), (PROJECT,), (OPEN, MARK), (OPEN, 1), (OPEN, 4), (OPEN, 5),
+    (PASS, 1, MARK), (MULTIPLY, 0, 0, 0), (TOKENS, 10), (PASS, 1, 0), (PASS, 1, 1), (PASS, 2, MARK),
+    (OPEN, 2), (OPEN, 3), (PASS, 2, 0), (PASS, 3, MARK), (PASS, 2, 1), (PASS, 1, 4), (PASS, 1, 5),
+    (PASS, 1, 2), (PASS, 1, 3), (PASS, 4, MARK), (READ,), (PASS, 3, 1), (TOKENS, 13), (TOKENS, 14),
+    (PASS, 3, 0), (MULTIPLY, 1, 0, 1), (MULTIPLY, 1, 0, 0), (MULTIPLY, 1, 1, 0), (PASS, 2, 4),
+    (PASS, 2, 5), (MULTIPLY, 0, 1, 0), (MULTIPLY, 1, 2, 0), (PASS, 2, 2), (PASS, 2, 3),
+    (MULTIPLY, 1, 2, 1), (PASS, 4, 1), (MULTIPLY, 0, 0, 1), (PASS, 4, 0), (MIX,), (TOKENS, 16),
+    (PASS, 3, 4), (PASS, 3, 5), (PASS, 3, 2), (PASS, 3, 3), (MULTIPLY, 0, 2, 1),
+    (MULTIPLY, 1, 3, 0), (MULTIPLY, 1, 1, 1), (MULTIPLY, 0, 1, 1), (MULTIPLY, 0, 3, 0),
+    (MULTIPLY, 0, 2, 0), (MULTIPLY, 1, 3, 1), (MULTIPLY, 0, 3, 1), (PASS, 4, 4), (PASS, 4, 5),
+    (PASS, 4, 2), (PASS, 4, 3), (MULTIPLY, 1, 4, 1), (MULTIPLY, 1, 4, 0), (MULTIPLY, 0, 4, 1),
+    (MULTIPLY, 0, 4, 0),
 )
 
 
@@ -63,10 +66,10 @@
 def kernel(
     dims,
     tokens, key_weight, value_weight, queries, head_offset, key_bias, own_bias,
-    kv, bias_out, packed,
-    tok, wts, acc, bias, query, offset, bias_all, bias_own, key_rows,
-    ubuf, ucat, pout, pin, plow, tot_out, tot_in,
-    local_sem, tok_load, sends, receives, ring_recv, last_recv, pair_recv, tok_recv,
+    kv, bias_out, packed, tok, wts, acc,
+    bias, query, offset, bias_all, bias_own, key_rows,
+    ubuf, ucat, pout, pin, plow, tot_out, tot_in, wout, win,
+    local_sem, tok_load, sends, receives, ring_recv, last_recv, pair_recv, tok_recv, ready,
 ):
     n, tp_count, seqs, pos, width, rows, cols, heads, head_dim, rows_h = dims
     hops = n // 2
@@ -89,6 +92,10 @@
         order.extend([-h, h] if h < hops else [h])
     chunk = width // n if chunked else width
     chunk_count = n if chunked else 1
+    early = min(EARLY_HOPS, hops - 1) if chunked else -1
+    cut = (2 * early + 1) * chunk if chunked else 0
+    tail = slice(cut, width)
+    crossing = 3 if chunked else 2
 
     def slot_of(step):
         if not chunked:
@@ -132,8 +139,16 @@
 
     tp_peers = [lax.rem(tp + k, tp_count) for k in range(1, tp_count)]
     barrier = pltpu.get_barrier_semaphore()
-    for target in ({"sp": right}, {"sp": left}, {"gr": partner}, *({"tp": p} for p in tp_peers)):
-        pl.semaphore_signal(barrier, inc=1, device_id=target, device_id_type=MESH)
+    ring = (right, left)
+
+    def signal(semaphore, target):
+        pl.semaphore_signal(semaphore, inc=1, device_id=target, device_id_type=MESH)
+
+    for target in ring:
+        pl.when(target > me)(functools.partial(signal, barrier, {"sp": target}))
+    pl.when(gr == 0)(functools.partial(signal, barrier, {"gr": partner}))
+    for peer in tp_peers:
+        pl.when(peer > tp)(functools.partial(signal, barrier, {"tp": peer}))
 
     def part_of(piece):
         return 1 if piece < VALUE_SUBS else 0
@@ -195,9 +210,14 @@
         )
 
     def read_move(k, which, source, target):
-        out, into = ((pout, pin), (tot_out, tot_in))[which]
+        if which == 0:
+            out, into = pout.at[target, :, tail], pin.at[source, :, tail]
+        elif which == 1:
+            out, into = tot_out.at[target], tot_in.at[source]
+        else:
+            out, into = wout.at[target], win.at[source]
         return pltpu.make_async_remote_copy(
-            src_ref=out.at[target], dst_ref=into.at[source],
+            src_ref=out, dst_ref=into,
             send_sem=sends.at[5 + which], recv_sem=receives.at[1 + which],
             device_id={"tp": peer_of(k)}, device_id_type=MESH,
         )
@@ -216,19 +236,35 @@
         else:
             counted(tok.at[:, my_rows, chunk:], tok_load.at[1]).wait()
 
-    def send_tokens(upto):
-        while issued[0] < min(upto, chunk_count * seqs):
-            i, s = divmod(issued[0], seqs)
-            if s == 0 and i < 2:
+    def send_tokens(upto, ahead=None):
+        upto = min(upto, chunk_count * seqs)
+        for i, s in (divmod(unit, seqs) for unit in range(issued[0], upto)):
+            if s == 0 and i < 2 and ahead is not True:
                 load_tokens(i)
             for k in range(tp_count - 1):
-                launch(tok_move(i, s, k, tp))
-            issued[0] += 1
-
-    def open_ring(piece):
+
+                def start(i=i, s=s, k=k):
+                    launch(tok_move(i, s, k, tp))
+
+                if ahead is None:
+                    start()
+                else:
+                    pl.when((peer_of(k) > tp) == ahead)(start)
+        if ahead is not False:
+            issued[0] = upto
+
+    def open_ring(piece, ahead=None):
         for direction in range(2):
-            if used(direction, 1, piece):
+            if not used(direction, 1, piece):
+                continue
+
+            def start(direction=direction):
                 launch(ring_copy(direction, 1, piece))
+
+            if ahead is None:
+                start()
+            else:
+                pl.when((ring[direction] > me) == ahead)(start)
 
     def pass_on(hop, piece):
         for direction in range(2):
@@ -254,6 +290,45 @@
         ubuf[slot_of(0)] = lax.dot_general(
             q_rows, key_rows[...], (((1,), (1,)), ((), ())), preferred_element_type=F32
         ).astype(BF16)
+
+    def greet():
+        behind = (right < me).astype(jnp.int32) + (left < me).astype(jnp.int32) + gr + tp
+        pl.when(behind > 0)(lambda: pl.semaphore_wait(barrier, behind))
+        for direction in range(2):
+            target = ring[direction]
+            semaphore = ready.at[1 - direction]
+            pl.when(target < me)(functools.partial(signal, semaphore, {"sp": target}))
+        pl.when(gr == 1)(functools.partial(signal, ready.at[2], {"gr": partner}))
+        for peer in tp_peers:
+            pl.when(peer < tp)(functools.partial(signal, ready.at[3], {"tp": peer}))
+
+    def begin(steps):
+        with jax.named_scope("greet"):
+            greet()
+        for kind, *what in steps:
+            if kind == OPEN:
+                if what[0] != MARK:
+                    weights_here(part_of(what[0]))
+                open_ring(what[0], False)
+            elif kind == TOKENS:
+                send_tokens(what[0], False)
+            elif kind == PROJECT:
+                with jax.named_scope("project"):
+                    project()
+        with jax.named_scope("ready"):
+            for direction in range(2):
+                semaphore = ready.at[direction]
+                pl.when(ring[direction] > me)(
+                    functools.partial(pl.semaphore_wait, semaphore, 1)
+                )
+            ahead = tp_count - 1 - tp
+            pl.when(ahead > 0)(lambda: pl.semaphore_wait(ready.at[3], ahead))
+        for kind, *what in steps:
+            if kind == OPEN:
+                open_ring(what[0], True)
+            elif kind == TOKENS:
+                send_tokens(what[0], True)
+        pl.when(gr == 0)(functools.partial(pl.semaphore_wait, ready.at[2], 1))
         bias_copy.wait()
         for k in range(tp_count - 1):
             launch(bias_move(k, tp, peer_of(k)))
@@ -299,18 +374,21 @@
         )
         m = seqs * group
         within = sums[:m] + sums[m : 2 * m] + sums[2 * m :]
-        weights = jnp.exp(taking + within).astype(BF16)
+        weights = jnp.exp(taking + within)
         totals = jnp.sum(fading, axis=1, keepdims=True)
         spread = jnp.broadcast_to(totals, (m, 128))
         weighted = [
             jnp.dot(
-                weights[s * group : (s + 1) * group], tok[s, my_rows, :],
+                weights[s * group : (s + 1) * group].astype(BF16), tok[s, my_rows, :],
                 preferred_element_type=F32,
             )
             for s in range(seqs)
         ]
         for t in range(tp_count):
             at = slice(t * rows_h, (t + 1) * rows_h)
+            wout[t] = jnp.concatenate(
+                [weights[s * group : (s + 1) * group][at] for s in range(seqs)], axis=0
+            ).astype(BF16)
             tot_out[t] = jnp.concatenate(
                 [spread[s * group + t * rows_h : s * group + (t + 1) * rows_h] for s in range(seqs)],
                 axis=0,
@@ -320,7 +398,7 @@
             pout[t] = upper
             plow[t] = (whole - upper.astype(F32)).astype(BF16)
         for k in range(tp_count - 1):
-            for which in range(2):
+            for which in range(crossing):
                 launch(read_move(k, which, tp, peer_of(k)))
         pin[tp] = pout[tp]
         tot_in[tp] = tot_out[tp]
@@ -378,20 +456,47 @@
             else:
                 kv[part, s] = y.astype(BF16)
 
+    def leave():
+        if chunked:
+            pair_ready(0, hops)
+            for s in range(seqs):
+                tokens_ready(hops, s)
+
     def mix_move(k, source):
         return pltpu.make_async_remote_copy(
             src_ref=packed.at[source], dst_ref=packed.at[source],
-            send_sem=sends.at[7], recv_sem=receives.at[3],
+            send_sem=sends.at[8], recv_sem=receives.at[4],
             device_id={"sp": lax.rem(me + k, n)}, device_id_type=MESH,
         )
 
     def mix():
         with jax.named_scope("await_products"):
             if tp_count > 1:
-                counted(pin.at[pl.ds(0, tp_count - 1)], receives.at[1]).wait()
-                counted(tot_in.at[pl.ds(0, tp_count - 1)], receives.at[2]).wait()
+                others = pl.ds(0, tp_count - 1)
+                counted(pin.at[others, :, tail], receives.at[1]).wait()
+                counted(tot_in.at[others], receives.at[2]).wait()
+                if chunked:
+                    counted(win.at[others], receives.at[3]).wait()
             for hop in range(1, hops + 1):
                 pair_ready(1, hop)
+        if chunked:
+            for h in range(early + 1):
+                for s in range(seqs):
+                    tokens_ready(h, s)
+            for k in range(tp_count - 1):
+                source = source_of(k)
+                where = pl.ds(pl.multiple_of(source * pos, pos), pos)
+                held = win[source].astype(F32)
+                pin[source, :, 0:cut] = jnp.concatenate(
+                    [
+                        jnp.dot(
+                            held[s * rows_h : (s + 1) * rows_h].astype(BF16),
+                            tok[s, where, 0:cut], preferred_element_type=F32,
+                        )
+                        for s in range(seqs)
+                    ],
+                    axis=0,
+                ).astype(BF16)
         count = seqs * rows_h
         given = jnp.concatenate([pin[t] for t in range(tp_count)] + [plow[tp]], axis=0)
         product = jnp.dot(
@@ -418,9 +523,10 @@
         for k in range(1, n):
             launch(mix_move(k, me))
 
-    with jax.named_scope("barrier"):
-        pl.semaphore_wait(barrier, 3 + len(tp_peers))
-    for kind, *what in plan(hops, seqs):
+    steps = list(plan(hops, seqs))
+    opening = next(i for i, step in enumerate(steps) if step[0] == PASS)
+    begin(steps[:opening])
+    for kind, *what in steps[opening:]:
         if kind == OPEN:
             if what[0] != MARK:
                 weights_here(part_of(what[0]))
@@ -431,10 +537,8 @@
         elif kind == TOKENS:
             send_tokens(what[0])
         elif kind == MULTIPLY:
-            multiply(*what)
-        elif kind == PROJECT:
-            with jax.named_scope("project"):
-                project()
+            if what[:2] != [0, hops]:
+                multiply(*what)
         elif kind == READ:
             with jax.named_scope("read"):
                 read()
@@ -442,6 +546,7 @@
             with jax.named_scope("mix"):
                 mix()
 
+    leave()
     if not chunked:
         for s in range(seqs):
             tokens_ready(0, s)
@@ -466,7 +571,7 @@
     for s in range(seqs):
         bias_out[s] = jnp.concatenate([bias[t, s] for t in range(tp_count)], axis=1)
     with jax.named_scope("await_mix"):
-        counted(packed.at[pl.ds(0, n - 1)], receives.at[3]).wait()
+        counted(packed.at[pl.ds(0, n - 1)], receives.at[4]).wait()
     with jax.named_scope("drain"):
         counted(wts.at[0, pl.ds(0, n - 1)], sends.at[0]).wait()
         counted(ubuf.at[pl.ds(0, n - 1)], sends.at[1]).wait()
@@ -475,19 +580,35 @@
             others = pl.ds(0, tp_count - 1)
             counted(tok.at[:, pl.ds(0, (tp_count - 1) * pos), :], sends.at[3]).wait()
             counted(bias.at[others], sends.at[4]).wait()
-            counted(pin.at[others], sends.at[5]).wait()
+            counted(pin.at[others, :, tail], sends.at[5]).wait()
             counted(tot_in.at[others], sends.at[6]).wait()
-        counted(packed.at[pl.ds(0, n - 1)], sends.at[7]).wait()
-
-
-def finish(n, head_dim, kv, bias, packed, key_out, value_out, bias_out, reading_out, sems):
+            if chunked:
+                counted(win.at[others], sends.at[7]).wait()
+        counted(packed.at[pl.ds(0, n - 1)], sends.at[8]).wait()
+
+
+def finish(
+    n, head_dim, kv, bias, packed, tok, wts, acc,
+    key_out, value_out, bias_out, reading_out, key, sems,
+):
+    _, _, rows, _ = wts.shape
+    chunked = rows % 128 == 0
     moves = [
-        pltpu.make_async_copy(kv.at[0], key_out, sems.at[0]),
-        pltpu.make_async_copy(kv.at[1], value_out, sems.at[1]),
-        pltpu.make_async_copy(bias, bias_out, sems.at[2]),
+        pltpu.make_async_copy(kv.at[1], value_out, sems.at[0]),
+        pltpu.make_async_copy(bias, bias_out, sems.at[1]),
     ]
+    if not chunked:
+        moves.append(pltpu.make_async_copy(kv.at[0], key_out, sems.at[2]))
     for c in moves:
         c.start()
+    if chunked:
+        for s in range(key_out.shape[0]):
+            y = jnp.dot(
+                tok[s, :, (n - 1) * rows :], wts[0, n - 1], preferred_element_type=F32
+            )
+            key[s] = (acc[0, s] + y).astype(BF16)
+            moves.append(pltpu.make_async_copy(key.at[s], key_out.at[s], sems.at[2 + s]))
+            moves[-1].start()
     seqs, cols = reading_out.shape
     rows_h = max(8, cols // head_dim)
     row_id = lax.broadcasted_iota(jnp.int32, (rows_h, cols), 0)
@@ -526,19 +647,19 @@
     dims = (n, tp_count, seqs, pos, width, rows, cols, heads, head_dim, rows_h)
     groups = hops + 1 if (width // n) % 128 == 0 else 1
     dma = pltpu.SemaphoreType.DMA
-    kv, bias_held, packed = pl.pallas_call(
+    kv, bias_held, packed, tok, wts, acc = pl.pallas_call(
         functools.partial(kernel, dims),
         out_shape=(
             jax.ShapeDtypeStruct((2, seqs, span, cols), BF16),
             jax.ShapeDtypeStruct((seqs, heads, span), BF16),
             jax.ShapeDtypeStruct((n, 2 * seqs, cols), F32),
+            jax.ShapeDtypeStruct((seqs, span, width), BF16),
+            jax.ShapeDtypeStruct((2, n, rows, cols), BF16),
+            jax.ShapeDtypeStruct((2, seqs, span, cols), F32),
         ),
         in_specs=[pl.BlockSpec(memory_space=pltpu.HBM)] * 7,
-        out_specs=[pl.BlockSpec(memory_space=pltpu.VMEM)] * 3,
+        out_specs=[pl.BlockSpec(memory_space=pltpu.VMEM)] * 6,
         scratch_shapes=[
-            pltpu.VMEM((seqs, span, width), BF16),
-            pltpu.VMEM((2, n, rows, cols), BF16),
-            pltpu.VMEM((2, seqs, span, cols), F32),
             pltpu.VMEM((tp_count, seqs, heads, pos), BF16),
             pltpu.VMEM(queries.shape, BF16),
             pltpu.VMEM((1, head_count), F32),
@@ -552,14 +673,17 @@
             pltpu.VMEM((tp_count, seqs * rows_h, width), BF16),
             pltpu.VMEM((tp_count, seqs * rows_h, 128), F32),
             pltpu.VMEM((tp_count, seqs * rows_h, 128), F32),
+            pltpu.VMEM((tp_count, seqs * rows_h, pos), BF16),
+            pltpu.VMEM((tp_count, seqs * rows_h, pos), BF16),
             dma((8,)),
             dma((2,)),
-            dma((8,)),
-            dma((4,)),
+            dma((9,)),
+            dma((5,)),
             dma((2, hops - 1, MARK + 1)),
             dma((MARK + 1,)),
             dma((2, hops)),
             dma((groups, seqs)),
+            pltpu.SemaphoreType.REGULAR((4,)),
         ],
         compiler_params=pltpu.CompilerParams(
             collective_id=0, has_side_effects=True, vmem_limit_bytes=36 * 2**20
@@ -577,7 +701,7 @@
         in_specs=[
             pl.BlockSpec(memory_space=pl.ANY),
             pl.BlockSpec(memory_space=pl.ANY),
-            pl.BlockSpec(memory_space=pltpu.VMEM),
+            *[pl.BlockSpec(memory_space=pltpu.VMEM)] * 4,
         ],
         out_specs=[
             pl.BlockSpec(memory_space=pl.ANY),
@@ -585,10 +709,10 @@
             pl.BlockSpec(memory_space=pl.ANY),
             pl.BlockSpec(memory_space=pltpu.VMEM),
         ],
-        scratch_shapes=[dma((3,))],
-        compiler_params=pltpu.CompilerParams(vmem_limit_bytes=4 * 2**20),
+        scratch_shapes=[pltpu.VMEM((seqs, span, cols), BF16), dma((2 + seqs,))],
+        compiler_params=pltpu.CompilerParams(vmem_limit_bytes=16 * 2**20),
         name="finish",
-    )(kv, bias_held, packed)
+    )(kv, bias_held, packed, tok, wts, acc)
     return key_cache, value_cache, jnp.transpose(bias_cache, (0, 2, 1)), reading
 
 

time: 34.3 us -> 33.2 us (0.968)
  Pallas kernels: 33.3 us -> 32.5 us
    pallas_call x1, Pallas kernels: 31.7 us -> 30.8 us  [per_device(): pl.pallas_call(functools.partial(kernel, dims), out_shape=(jax.ShapeDtype...]
where the time goes in v4:
time: 33.2 us; the launch traced here: 33.1 us
  Pallas kernels  32.5 us (98%)
  between operations  0.64 us (2%)
    pallas_call x1, Pallas kernels, per_device(): pl.pallas_call(functools.partial(kernel, dims), out_shape=(jax.ShapeDtype...  30.8 us
    pallas_call x1, Pallas kernels, per_device(): pl.pallas_call(functools.partial(finish, n, head_dim), out_shape=(jax.Sha...  1.66 us

profile of v4, /device:TPU:0, one launch (start us, length us, event | category | flops | bytes accessed | tf_op | source)
XLA Modules:
  0.0 33.1 jit_solution(11475991019964480614)
XLA Ops:
  0.6 30.8 %prefill.1 = (bf16[2,2,256,512]{3,2,1,0:T(8,128)(2,1)S(1)}, bf16[2,8,256]{2,1,0:T(8,128)(2,1)S(1)}, f32[8,4,512]{2,1,0:T(4,128)S(1)}, bf16[2,256,2048]{2,1,0:T(8...) custom-call(bf16[2,128,2048]{2,1,0:T(8,128)(2,1)} %tokens.1, ...), custom_call_target="tpu_custom_call" | custom-call | tf_op jit(solution)/shard_map/prefill/pallas_call | solution.py:650
  31.4 1.7 %finish.1 = (bf16[2,256,512]{2,1,0:T(8,128)(2,1)}, bf16[2,256,512]{2,1,0:T(8,128)(2,1)}, bf16[2,8,256]{2,1,0:T(8,128)(2,1)}, f32[2,512]{1,0:T(2,128)}) custom-call(bf16[2,2,256,512]{3,2,1,0:T(8,128)(2,1)S(1)} %get-tuple-element.14.kv, bf16[2,8,256]{2,1,0:T(8,128)(2,1)S(1)} %get-tuple-element.15.bias, f32[8,4,512]{2,1,0:T(4,128)S(1)} %get-tuple-element.16.packed, ...), custom_call_target="tpu_custom_call" | custom-call | tf_op jit(solution)/shard_map/finish/pallas_call | solution.py:693

commit v5 on v4

--- a/solution.py
+++ b/solution.py
@@ -37,18 +37,18 @@
 
 
 TUNED = (
-    (OPEN, 0), (TOKENS, 6), (PROJECT,), (OPEN, MARK), (OPEN, 1), (OPEN, 4), (OPEN, 5),
-    (PASS, 1, MARK), (MULTIPLY, 0, 0, 0), (TOKENS, 10), (PASS, 1, 0), (PASS, 1, 1), (PASS, 2, MARK),
-    (OPEN, 2), (OPEN, 3), (PASS, 2, 0), (PASS, 3, MARK), (PASS, 2, 1), (PASS, 1, 4), (PASS, 1, 5),
-    (PASS, 1, 2), (PASS, 1, 3), (PASS, 4, MARK), (READ,), (PASS, 3, 1), (TOKENS, 13), (TOKENS, 14),
-    (PASS, 3, 0), (MULTIPLY, 1, 0, 1), (MULTIPLY, 1, 0, 0), (MULTIPLY, 1, 1, 0), (PASS, 2, 4),
-    (PASS, 2, 5), (MULTIPLY, 0, 1, 0), (MULTIPLY, 1, 2, 0), (PASS, 2, 2), (PASS, 2, 3),
-    (MULTIPLY, 1, 2, 1), (PASS, 4, 1), (MULTIPLY, 0, 0, 1), (PASS, 4, 0), (MIX,), (TOKENS, 16),
-    (PASS, 3, 4), (PASS, 3, 5), (PASS, 3, 2), (PASS, 3, 3), (MULTIPLY, 0, 2, 1),
-    (MULTIPLY, 1, 3, 0), (MULTIPLY, 1, 1, 1), (MULTIPLY, 0, 1, 1), (MULTIPLY, 0, 3, 0),
-    (MULTIPLY, 0, 2, 0), (MULTIPLY, 1, 3, 1), (MULTIPLY, 0, 3, 1), (PASS, 4, 4), (PASS, 4, 5),
-    (PASS, 4, 2), (PASS, 4, 3), (MULTIPLY, 1, 4, 1), (MULTIPLY, 1, 4, 0), (MULTIPLY, 0, 4, 1),
-    (MULTIPLY, 0, 4, 0),
+    (OPEN, 0), (TOKENS, 10), (PROJECT,), (OPEN, MARK), (OPEN, 1), (OPEN, 4), (PASS, 1, MARK),
+    (OPEN, 3), (PASS, 1, 0), (PASS, 1, 1), (PASS, 2, MARK), (OPEN, 2), (OPEN, 5), (PASS, 2, 0),
+    (PASS, 3, MARK), (MULTIPLY, 0, 0, 0), (PASS, 2, 1), (PASS, 1, 2), (PASS, 1, 4), (PASS, 1, 5),
+    (PASS, 4, MARK), (PASS, 1, 3), (MULTIPLY, 1, 0, 0), (READ,), (PASS, 3, 0), (MULTIPLY, 1, 1, 0),
+    (PASS, 3, 1), (TOKENS, 13), (TOKENS, 14), (MULTIPLY, 0, 1, 0), (PASS, 2, 4), (PASS, 2, 2),
+    (MULTIPLY, 1, 2, 0), (MULTIPLY, 0, 0, 1), (PASS, 2, 5), (MULTIPLY, 1, 0, 1), (TOKENS, 16),
+    (MULTIPLY, 1, 2, 1), (PASS, 2, 3), (PASS, 4, 1), (PASS, 4, 0), (MIX,), (PASS, 3, 4),
+    (MULTIPLY, 1, 1, 1), (PASS, 3, 5), (PASS, 3, 2), (PASS, 3, 3), (MULTIPLY, 0, 2, 0),
+    (MULTIPLY, 1, 3, 0), (MULTIPLY, 0, 3, 0), (MULTIPLY, 0, 3, 1), (MULTIPLY, 0, 2, 1),
+    (PASS, 4, 4), (MULTIPLY, 1, 3, 1), (PASS, 4, 2), (PASS, 4, 5), (PASS, 4, 3),
+    (MULTIPLY, 0, 1, 1), (MULTIPLY, 1, 4, 0), (MULTIPLY, 1, 4, 1), (MULTIPLY, 0, 4, 0),
+    (MULTIPLY, 0, 4, 1),
 )
 
 
@@ -589,7 +589,7 @@
 
 def finish(
     n, head_dim, kv, bias, packed, tok, wts, acc,
-    key_out, value_out, bias_out, reading_out, key, sems,
+    key_out, value_out, bias_out, reading_out, key, reading, sems,
 ):
     _, _, rows, _ = wts.shape
     chunked = rows % 128 == 0
@@ -607,7 +607,7 @@
                 tok[s, :, (n - 1) * rows :], wts[0, n - 1], preferred_element_type=F32
             )
             key[s] = (acc[0, s] + y).astype(BF16)
-            moves.append(pltpu.make_async_copy(key.at[s], key_out.at[s], sems.at[2 + s]))
+            moves.append(pltpu.make_async_copy(key.at[s], key_out.at[s], sems.at[4 + s]))
             moves[-1].start()
     seqs, cols = reading_out.shape
     rows_h = max(8, cols // head_dim)
@@ -623,7 +623,9 @@
         x = mixture[s : s + 1]
         mean = jnp.sum(jnp.where(own, x * x, 0.0), axis=1, keepdims=True) / head_dim
         scale = jnp.sum(jnp.where(own, lax.rsqrt(mean + 1e-06), 0.0), axis=0, keepdims=True)
-        reading_out[s : s + 1] = x * scale
+        reading[s : s + 1] = x * scale
+    moves.append(pltpu.make_async_copy(reading, reading_out, sems.at[3]))
+    moves[-1].start()
     for c in moves:
         c.wait()
 
@@ -707,9 +709,11 @@
             pl.BlockSpec(memory_space=pl.ANY),
             pl.BlockSpec(memory_space=pl.ANY),
             pl.BlockSpec(memory_space=pl.ANY),
-            pl.BlockSpec(memory_space=pltpu.VMEM),
+            pl.BlockSpec(memory_space=pl.ANY),
         ],
-        scratch_shapes=[pltpu.VMEM((seqs, span, cols), BF16), dma((2 + seqs,))],
+        scratch_shapes=[
+            pltpu.VMEM((seqs, span, cols), BF16), pltpu.VMEM((seqs, cols), F32), dma((4 + seqs,))
+        ],
         compiler_params=pltpu.CompilerParams(vmem_limit_bytes=16 * 2**20),
         name="finish",
     )(kv, bias_held, packed, tok, wts, acc)

time: 33.2 us -> 32.9 us (level)
  Pallas kernels: 32.5 us -> 32.1 us
    pallas_call x1, Pallas kernels: 1.66 us -> 1.09 us  [per_device(): pl.pallas_call(functools.partial(finish, n, head_dim), out_shape=(jax.Sha...]
where the time goes in v5:
time: 32.9 us; the launch traced here: 32.7 us
  Pallas kernels  32.1 us (98%)
  between operations  0.64 us (2%)
    pallas_call x1, Pallas kernels, per_device(): pl.pallas_call(functools.partial(kernel, dims), out_shape=(jax.ShapeDtype...  31 us
    pallas_call x1, Pallas kernels, per_device(): pl.pallas_call(functools.partial(finish, n, head_dim), out_shape=(jax.Sha...  1.09 us

profile of v5, /device:TPU:0, one launch (start us, length us, event | category | flops | bytes accessed | tf_op | source)
XLA Modules:
  0.0 32.7 jit_solution(12982968174634813372)
XLA Ops:
  0.6 31.0 %prefill.1 = (bf16[2,2,256,512]{3,2,1,0:T(8,128)(2,1)S(1)}, bf16[2,8,256]{2,1,0:T(8,128)(2,1)S(1)}, f32[8,4,512]{2,1,0:T(4,128)S(1)}, bf16[2,256,2048]{2,1,0:T(8...) custom-call(bf16[2,128,2048]{2,1,0:T(8,128)(2,1)} %tokens.1, ...), custom_call_target="tpu_custom_call" | custom-call | tf_op jit(solution)/shard_map/prefill/pallas_call | solution.py:652
  31.6 1.1 %finish.1 = (bf16[2,256,512]{2,1,0:T(8,128)(2,1)}, bf16[2,256,512]{2,1,0:T(8,128)(2,1)}, bf16[2,8,256]{2,1,0:T(8,128)(2,1)}, f32[2,512]{1,0:T(2,128)}) custom-call(bf16[2,2,256,512]{3,2,1,0:T(8,128)(2,1)S(1)} %get-tuple-element.14.kv, bf16[2,8,256]{2,1,0:T(8,128)(2,1)S(1)} %get-tuple-element.15.bias, f32[8,4,512]{2,1,0:T(4,128)S(1)} %get-tuple-element.16.packed, ...), custom_call_target="tpu_custom_call" | custom-call | tf_op jit(solution)/shard_map/finish/pallas_call | solution.py:695

commit v6 on v4

--- a/solution.py
+++ b/solution.py
@@ -40,14 +40,14 @@
     (OPEN, 0), (TOKENS, 6), (PROJECT,), (OPEN, MARK), (OPEN, 1), (OPEN, 4), (OPEN, 5),
     (PASS, 1, MARK), (MULTIPLY, 0, 0, 0), (TOKENS, 10), (PASS, 1, 0), (PASS, 1, 1), (PASS, 2, MARK),
     (OPEN, 2), (OPEN, 3), (PASS, 2, 0), (PASS, 3, MARK), (PASS, 2, 1), (PASS, 1, 4), (PASS, 1, 5),
-    (PASS, 1, 2), (PASS, 1, 3), (PASS, 4, MARK), (READ,), (PASS, 3, 1), (TOKENS, 13), (TOKENS, 14),
+    (PASS, 1, 2), (PASS, 1, 3), (PASS, 4, MARK), (READ,), (PASS, 3, 1), (TOKENS, 13), (TOKENS, 15),
     (PASS, 3, 0), (MULTIPLY, 1, 0, 1), (MULTIPLY, 1, 0, 0), (MULTIPLY, 1, 1, 0), (PASS, 2, 4),
     (PASS, 2, 5), (MULTIPLY, 0, 1, 0), (MULTIPLY, 1, 2, 0), (PASS, 2, 2), (PASS, 2, 3),
     (MULTIPLY, 1, 2, 1), (PASS, 4, 1), (MULTIPLY, 0, 0, 1), (PASS, 4, 0), (MIX,), (TOKENS, 16),
     (PASS, 3, 4), (PASS, 3, 5), (PASS, 3, 2), (PASS, 3, 3), (MULTIPLY, 0, 2, 1),
-    (MULTIPLY, 1, 3, 0), (MULTIPLY, 1, 1, 1), (MULTIPLY, 0, 1, 1), (MULTIPLY, 0, 3, 0),
+    (MULTIPLY, 0, 1, 1), (MULTIPLY, 0, 3, 0), (MULTIPLY, 1, 3, 0), (MULTIPLY, 1, 1, 1),
     (MULTIPLY, 0, 2, 0), (MULTIPLY, 1, 3, 1), (MULTIPLY, 0, 3, 1), (PASS, 4, 4), (PASS, 4, 5),
-    (PASS, 4, 2), (PASS, 4, 3), (MULTIPLY, 1, 4, 1), (MULTIPLY, 1, 4, 0), (MULTIPLY, 0, 4, 1),
+    (PASS, 4, 2), (PASS, 4, 3), (MULTIPLY, 1, 4, 0), (MULTIPLY, 1, 4, 1), (MULTIPLY, 0, 4, 1),
     (MULTIPLY, 0, 4, 0),
 )
 
@@ -169,7 +169,7 @@
             src_ref=block_of(piece, step_of(direction, hop - 1), gr),
             dst_ref=block_of(piece, step_of(direction, hop), gr),
             send_sem=sends.at[1 if piece == MARK else 0],
-            recv_sem=(last_recv.at[piece] if hop == hops else ring_recv.at[direction, hop - 1, piece]),
+            recv_sem=(last_recv.at[piece] if hop == hops else ring_recv.at[hop - 1, piece]),
             device_id={"sp": right if direction == 0 else left}, device_id_type=MESH,
         )
 
@@ -266,11 +266,22 @@
             else:
                 pl.when((ring[direction] > me) == ahead)(start)
 
+    def arrived(hop, piece):
+        if hop == hops:
+            last = next(d for d in range(2) if used(d, hop, piece))
+            ring_copy(last, hop, piece).wait_recv()
+        elif piece == MARK:
+            counted(ubuf.at[pl.ds(0, 2)], ring_recv.at[hop - 1, piece]).wait()
+        else:
+            part = part_of(piece)
+            both = 2 * (half_rows // (VALUE_SUBS if part == 1 else KEY_SUBS))
+            counted(wts.at[part, 0, pl.ds(0, both)], ring_recv.at[hop - 1, piece]).wait()
+
     def pass_on(hop, piece):
+        arrived(hop, piece)
         for direction in range(2):
             if not used(direction, hop, piece):
                 continue
-            ring_copy(direction, hop, piece).wait_recv()
             if hop < hops and used(direction, hop + 1, piece):
                 launch(ring_copy(direction, hop + 1, piece))
             if piece != MARK:
@@ -589,7 +600,7 @@
 
 def finish(
     n, head_dim, kv, bias, packed, tok, wts, acc,
-    key_out, value_out, bias_out, reading_out, key, sems,
+    key_out, value_out, bias_out, reading_out, key, reading, sems,
 ):
     _, _, rows, _ = wts.shape
     chunked = rows % 128 == 0
@@ -607,7 +618,7 @@
                 tok[s, :, (n - 1) * rows :], wts[0, n - 1], preferred_element_type=F32
             )
             key[s] = (acc[0, s] + y).astype(BF16)
-            moves.append(pltpu.make_async_copy(key.at[s], key_out.at[s], sems.at[2 + s]))
+            moves.append(pltpu.make_async_copy(key.at[s], key_out.at[s], sems.at[4 + s]))
             moves[-1].start()
     seqs, cols = reading_out.shape
     rows_h = max(8, cols // head_dim)
@@ -623,7 +634,9 @@
         x = mixture[s : s + 1]
         mean = jnp.sum(jnp.where(own, x * x, 0.0), axis=1, keepdims=True) / head_dim
         scale = jnp.sum(jnp.where(own, lax.rsqrt(mean + 1e-06), 0.0), axis=0, keepdims=True)
-        reading_out[s : s + 1] = x * scale
+        reading[s : s + 1] = x * scale
+    moves.append(pltpu.make_async_copy(reading, reading_out, sems.at[3]))
+    moves[-1].start()
     for c in moves:
         c.wait()
 
@@ -679,7 +692,7 @@
             dma((2,)),
             dma((9,)),
             dma((5,)),
-            dma((2, hops - 1, MARK + 1)),
+            dma((hops - 1, MARK + 1)),
             dma((MARK + 1,)),
             dma((2, hops)),
             dma((groups, seqs)),
@@ -707,9 +720,11 @@
             pl.BlockSpec(memory_space=pl.ANY),
             pl.BlockSpec(memory_space=pl.ANY),
             pl.BlockSpec(memory_space=pl.ANY),
-            pl.BlockSpec(memory_space=pltpu.VMEM),
+            pl.BlockSpec(memory_space=pl.ANY),
         ],
-        scratch_shapes=[pltpu.VMEM((seqs, span, cols), BF16), dma((2 + seqs,))],
+        scratch_shapes=[
+            pltpu.VMEM((seqs, span, cols), BF16), pltpu.VMEM((seqs, cols), F32), dma((4 + seqs,))
+        ],
         compiler_params=pltpu.CompilerParams(vmem_limit_bytes=16 * 2**20),
         name="finish",
     )(kv, bias_held, packed, tok, wts, acc)

time: 33.2 us -> 32.5 us (0.979)
  Pallas kernels: 32.5 us -> 31.7 us
    pallas_call x1, Pallas kernels: 1.66 us -> 1.1 us  [per_device(): pl.pallas_call(functools.partial(finish, n, head_dim), out_shape=(jax.Sha...]
where the time goes in v6:
time: 32.5 us; the launch traced here: 32.3 us
  Pallas kernels  31.7 us (98%)
  between operations  0.64 us (2%)
    pallas_call x1, Pallas kernels, per_device(): pl.pallas_call(functools.partial(kernel, dims), out_shape=(jax.ShapeDtype...  30.6 us
    pallas_call x1, Pallas kernels, per_device(): pl.pallas_call(functools.partial(finish, n, head_dim), out_shape=(jax.Sha...  1.1 us

profile of v6, /device:TPU:0, one launch (start us, length us, event | category | flops | bytes accessed | tf_op | source)
XLA Modules:
  0.0 32.3 jit_solution(6330072716729467074)
XLA Ops:
  0.6 30.6 %prefill.1 = (bf16[2,2,256,512]{3,2,1,0:T(8,128)(2,1)S(1)}, bf16[2,8,256]{2,1,0:T(8,128)(2,1)S(1)}, f32[8,4,512]{2,1,0:T(4,128)S(1)}, bf16[2,256,2048]{2,1,0:T(8...) custom-call(bf16[2,128,2048]{2,1,0:T(8,128)(2,1)} %tokens.1, ...), custom_call_target="tpu_custom_call" | custom-call | tf_op jit(solution)/shard_map/prefill/pallas_call | solution.py:663
  31.2 1.1 %finish.1 = (bf16[2,256,512]{2,1,0:T(8,128)(2,1)}, bf16[2,256,512]{2,1,0:T(8,128)(2,1)}, bf16[2,8,256]{2,1,0:T(8,128)(2,1)}, f32[2,512]{1,0:T(2,128)}) custom-call(bf16[2,2,256,512]{3,2,1,0:T(8,128)(2,1)S(1)} %get-tuple-element.14.kv, bf16[2,8,256]{2,1,0:T(8,128)(2,1)S(1)} %get-tuple-element.15.bias, f32[8,4,512]{2,1,0:T(4,128)S(1)} %get-tuple-element.16.packed, ...), custom_call_target="tpu_custom_call" | custom-call | tf_op jit(solution)/shard_map/finish/pallas_call | solution.py:706

commit v7 on v6

--- a/solution.py
+++ b/solution.py
@@ -198,7 +198,7 @@
         block = tok.at[s, place_rows, columns(i)]
         return pltpu.make_async_remote_copy(
             src_ref=block, dst_ref=block,
-            send_sem=sends.at[3], recv_sem=tok_recv.at[(i + 1) // 2 if chunked else 0, s],
+            send_sem=sends.at[3], recv_sem=tok_recv.at[(i + 1) // 2 if chunked else 0],
             device_id={"tp": peer_of(k)}, device_id_type=MESH,
         )
 
@@ -431,13 +431,13 @@
         counted(held, pair_recv.at[part, hop - 1]).wait()
 
     def tokens_ready(hop, s):
-        if ("tok", hop, s) in seen or tp_count == 1:
+        if ("tok", hop) in seen or tp_count == 1:
             return
-        seen.add(("tok", hop, s))
+        seen.add(("tok", hop))
         first, end = slots_of_hop(hop) if chunked else (0, 1)
         counted(
-            tok.at[s, pl.ds(0, (tp_count - 1) * pos), slice(first * chunk, end * chunk)],
-            tok_recv.at[hop, s],
+            tok.at[:, pl.ds(0, (tp_count - 1) * pos), slice(first * chunk, end * chunk)],
+            tok_recv.at[hop],
         ).wait()
 
     def slots_of_hop(hop):
@@ -695,7 +695,7 @@
             dma((hops - 1, MARK + 1)),
             dma((MARK + 1,)),
             dma((2, hops)),
-            dma((groups, seqs)),
+            dma((groups,)),
             pltpu.SemaphoreType.REGULAR((4,)),
         ],
         compiler_params=pltpu.CompilerParams(

time: 32.5 us -> 33 us (1.015)
  Pallas kernels: 31.7 us -> 32.2 us
    pallas_call x1, Pallas kernels: 30.6 us -> 31.1 us  [per_device(): pl.pallas_call(functools.partial(kernel, dims), out_shape=(jax.ShapeDtype...]
where the time goes in v7:
time: 33 us; the launch traced here: 32.8 us
  Pallas kernels  32.2 us (98%)
  between operations  0.64 us (2%)
    pallas_call x1, Pallas kernels, per_device(): pl.pallas_call(functools.partial(kernel, dims), out_shape=(jax.ShapeDtype...  31.1 us
    pallas_call x1, Pallas kernels, per_device(): pl.pallas_call(functools.partial(finish, n, head_dim), out_shape=(jax.Sha...  1.09 us

profile of v7, /device:TPU:0, one launch (start us, length us, event | category | flops | bytes accessed | tf_op | source)
XLA Modules:
  0.0 32.8 jit_solution(16877779292429612344)
XLA Ops:
  0.6 31.1 %prefill.1 = (bf16[2,2,256,512]{3,2,1,0:T(8,128)(2,1)S(1)}, bf16[2,8,256]{2,1,0:T(8,128)(2,1)S(1)}, f32[8,4,512]{2,1,0:T(4,128)S(1)}, bf16[2,256,2048]{2,1,0:T(8...) custom-call(bf16[2,128,2048]{2,1,0:T(8,128)(2,1)} %tokens.1, ...), custom_call_target="tpu_custom_call" | custom-call | tf_op jit(solution)/shard_map/prefill/pallas_call | solution.py:663
  31.7 1.1 %finish.1 = (bf16[2,256,512]{2,1,0:T(8,128)(2,1)}, bf16[2,256,512]{2,1,0:T(8,128)(2,1)}, bf16[2,8,256]{2,1,0:T(8,128)(2,1)}, f32[2,512]{1,0:T(2,128)}) custom-call(bf16[2,2,256,512]{3,2,1,0:T(8,128)(2,1)S(1)} %get-tuple-element.14.kv, bf16[2,8,256]{2,1,0:T(8,128)(2,1)S(1)} %get-tuple-element.15.bias, f32[8,4,512]{2,1,0:T(4,128)S(1)} %get-tuple-element.16.packed, ...), custom_call_target="tpu_custom_call" | custom-call | tf_op jit(solution)/shard_map/finish/pallas_call | solution.py:706
